TPU v7x, 32 devices: a whole 2x2x4 slice. The times are simulated.
32 devices in a mesh: grp: 2 (over y), sp: 4 (over z), tp: 4 (over x, core).
Axes of the slice: x: 2, y: 2, z: 4, core: 2. Of those that a mesh axis runs over, the one named last changes fastest.
Arguments:
- tokens: bfloat16 [1024, 2048], P(('grp', 'sp'), 'tp'), parts along dimension 0
- mix_gain: bfloat16 [2048], replicated, may hold values from 0.099609375 to 1.8984375
- w_conv_value: bfloat16 [2048, 1024], P('sp', 'tp'), may hold values from -0.125 to 0.125
- w_conv_outer: bfloat16 [2048, 1024], P('sp', 'tp'), may hold values from -0.125 to 0.125
- w_conv_inner: bfloat16 [2048, 1024], P('sp', 'tp'), may hold values from -0.125 to 0.125
- conv_kernel: bfloat16 [3, 1024], P(None, 'tp'), may hold values from -3.5 to 3.5
- w_q_down: bfloat16 [2048, 512], P(None, 'tp'), may hold values from -0.125 to 0.125
- w_kv_down: bfloat16 [2048, 256], P(None, 'tp'), may hold values from -0.125 to 0.125
- w_rope_key: bfloat16 [2048, 32], replicated, may hold values from -0.125 to 0.125
- q_gain: bfloat16 [512], replicated
- kv_gain: bfloat16 [256], replicated, may hold values from 0.099609375 to 1.8984375
- w_q_nope: bfloat16 [512, 1024], P(None, 'tp'), may hold values from -0.25 to 0.25
- w_q_rope: bfloat16 [512, 512], P(None, 'tp'), may hold values from -0.25 to 0.25
- w_k_nope: bfloat16 [256, 1024], P(None, 'tp'), may hold values from -0.375 to 0.375
- w_value: bfloat16 [256, 1024], P(None, 'tp'), may hold values from -0.375 to 0.375
- w_out_conv: bfloat16 [1024, 2048], P('tp'), may hold values from -0.1875 to 0.1875
- w_out_attn: bfloat16 [1024, 2048], P('tp'), may hold values from -1.5 to 1.5
Outputs:
- mixed: bfloat16 [1024, 2048], P(('grp', 'sp'), 'tp'), parts along dimension 0
There are 2 independent parts, one for each index of `grp`. A program takes and returns all parts, laid end to end along the dimension named above; an argument that names none is the same for every part. Nothing has to cross between parts.
All inputs are finite; a program needn't handle non-finite values.
Results may differ from a plain program's by a relative error of at most 0.028.
Values may be sent and summed in bfloat16 or wider, within the bound.
A program may use at most 64 MiB of HBM per device.

v0:
```python
import functools

import jax
import jax.numpy as jnp
import numpy as np
from jax import lax
from jax.experimental import pallas as pl
from jax.experimental.pallas import tpu as pltpu
from jax.sharding import PartitionSpec as P

MESH = pl.DeviceIdType.MESH

D = 2048
NOPE = 64
ROPE = 32
VALUE = 64


EPS = 1e-06
THETA = 10000.0


def with_halo(x, sides, width):
    for axis, dim in sides:
        size, length = (lax.axis_size(axis), x.shape[dim])
        up = [(i, (i + 1) % size) for i in range(size - 1)]
        down = [(j, i) for i, j in up]
        last = lax.slice_in_dim(x, length - width, length, axis=dim)
        first = lax.slice_in_dim(x, 0, width, axis=dim)
        before = lax.ppermute(last, axis, up)
        after = lax.ppermute(first, axis, down)
        x = jnp.concatenate([before, x, after], axis=dim)
    return x


def rms_scale(values):
    return lax.rsqrt(jnp.mean(values * values, axis=-1, keepdims=True) + EPS)


def angles(positions, width):
    inverse = THETA ** (-jnp.arange(0, width, 2, dtype=jnp.float32) / width)
    phase = positions[:, None] * inverse[None, :]
    phase = jnp.concatenate([phase, phase], axis=-1)
    return (jnp.cos(phase), jnp.sin(phase))


def turned(values, cosine, sine):
    half = values.shape[-1] // 2
    first = values[..., :half]
    second = values[..., half:]
    return values * cosine + jnp.concatenate([-second, first], axis=-1) * sine


def block_rows(count):
    for candidate in range(min(count, 1024), 0, -1):
        if count % candidate == 0 and candidate % 128 == 0:
            return candidate
    for candidate in range(min(count, 1024), 0, -1):
        if count % candidate == 0:
            return candidate
    return count


def gathered_weights(
    tokens,
    mix_gain,
    w_conv_value,
    w_conv_outer,
    w_conv_inner,
    conv_kernel,
    w_q_down,
    w_kv_down,
    w_rope_key,
    q_gain,
    kv_gain,
    w_q_nope,
    w_q_rope,
    w_k_nope,
    w_value,
    w_out_conv,
    w_out_attn,
):
    f32 = jnp.float32
    bf16 = jnp.bfloat16
    rows = tokens.shape[0]
    conv_value_w, conv_outer_w, conv_inner_w = (
        lax.all_gather(w_conv_value, "sp", axis=0, tiled=True),
        lax.all_gather(w_conv_outer, "sp", axis=0, tiled=True),
        lax.all_gather(w_conv_inner, "sp", axis=0, tiled=True),
    )
    matrices = (conv_value_w, conv_outer_w, conv_inner_w, w_q_down, w_kv_down, w_rope_key)
    gain = mix_gain.astype(f32)
    piece_f = lax.all_gather(tokens, "tp", axis=1, tiled=True).astype(f32)
    scaled = (piece_f * gain).astype(bf16)
    updated = tuple((jnp.dot(scaled, matrix, preferred_element_type=f32) for matrix in matrices))
    squares = jnp.sum(piece_f * piece_f, axis=1)
    row_scale = lax.rsqrt(squares / D + EPS)[:, None]
    conv_value, conv_outer, conv_inner, q_part, kv_part, rope_raw = [
        (row_scale * total).astype(bf16) for total in updated
    ]
    gated = (conv_inner.astype(f32) * conv_value.astype(f32)).astype(bf16)
    padded = with_halo(gated, (("sp", 0),), 1).astype(f32)
    kernel = conv_kernel.astype(f32)
    conv_out = padded[:-2] * kernel[0] + padded[1:-1] * kernel[1] + padded[2:] * kernel[2]
    y_conv = (conv_outer.astype(f32) * conv_out).astype(bf16)
    q_latent, kv_latent = (
        lax.all_gather(q_part, "tp", axis=1, tiled=True),
        lax.all_gather(kv_part, "tp", axis=1, tiled=True),
    )
    q_float = q_latent.astype(f32)
    q_normed = (q_float * rms_scale(q_float) * q_gain.astype(f32)).astype(bf16)
    kv_float = kv_latent.astype(f32)
    kv_normed = (kv_float * rms_scale(kv_float) * kv_gain.astype(f32)).astype(bf16)
    heads = w_q_nope.shape[1] // NOPE
    positions = (lax.axis_index("sp") * rows + jnp.arange(rows, dtype=jnp.int32)).astype(f32)
    cosine, sine = angles(positions, ROPE)
    q_nope = (
        jnp.dot(q_normed, w_q_nope, preferred_element_type=f32)
        .astype(bf16)
        .reshape(rows, heads, NOPE)
    )
    q_rope_raw = jnp.dot(q_normed, w_q_rope, preferred_element_type=f32).reshape(rows, heads, ROPE)
    q_rope = turned(q_rope_raw, cosine[:, None, :], sine[:, None, :]).astype(bf16)
    k_rope = turned(rope_raw.astype(f32), cosine, sine).astype(bf16)
    factor = (NOPE + ROPE) ** (-0.5)

    def attend(state, key_block, value_block, rope_block):
        peak, total, summed = state
        count = key_block.shape[0]
        keys3 = key_block.reshape(count, heads, NOPE)
        values3 = value_block.reshape(count, heads, VALUE)
        scores = jnp.einsum("qhd,khd->qhk", q_nope, keys3, preferred_element_type=f32)
        scores = scores + jnp.einsum("qhr,kr->qhk", q_rope, rope_block, preferred_element_type=f32)
        scores = scores * factor
        new_peak = jnp.maximum(peak, jnp.max(scores, axis=-1))
        fade = jnp.exp(peak - new_peak)
        weights = jnp.exp(scores - new_peak[..., None])
        total = total * fade + jnp.sum(weights, axis=-1)
        summed = summed * fade[..., None] + jnp.einsum(
            "qhk,khd->qhd", weights.astype(bf16), values3, preferred_element_type=f32
        )
        return (new_peak, total, summed)

    start_state = (
        jnp.full((rows, heads), -jnp.inf, f32),
        jnp.zeros((rows, heads), f32),
        jnp.zeros((rows, heads, VALUE), f32),
    )
    latent = lax.all_gather(kv_normed, "sp", axis=0, tiled=True)
    rope_keys = lax.all_gather(k_rope, "sp", axis=0, tiled=True)
    size = block_rows(latent.shape[0])
    count = latent.shape[0] // size

    def one_block(carry, blocks):
        latent_block, rope_block = blocks
        key_block = jnp.dot(latent_block, w_k_nope, preferred_element_type=f32).astype(bf16)
        value_block = jnp.dot(latent_block, w_value, preferred_element_type=f32).astype(bf16)
        return (attend(carry, key_block, value_block, rope_block), None)

    carry, ignored = lax.scan(
        one_block,
        start_state,
        (
            latent.reshape(count, size, latent.shape[1]),
            rope_keys.reshape(count, size, rope_keys.shape[1]),
        ),
    )
    peak, total, summed = carry
    y_attn = (summed / total[..., None]).astype(bf16).reshape(rows, heads * VALUE)
    partial_sum = jnp.dot(y_conv, w_out_conv, preferred_element_type=f32) + jnp.dot(
        y_attn, w_out_attn, preferred_element_type=f32
    )
    return (
        lax.psum_scatter(partial_sum.astype(jnp.bfloat16), "tp", scatter_dimension=1, tiled=True)
        .astype(jnp.float32)
        .astype(bf16)
    )


def copy_to(src, dst, send, recv, sp, tp):
    return pltpu.make_async_remote_copy(
        src_ref=src,
        dst_ref=dst,
        send_sem=send,
        recv_sem=recv,
        device_id={"sp": sp, "tp": tp},
        device_id_type=MESH,
    )


def dot(a, b):
    return jnp.dot(a, b, preferred_element_type=jnp.float32)


def dot_t(a, b):
    return lax.dot_general(a, b, (((1,), (1,)), ((), ())), preferred_element_type=jnp.float32)


def mixer_kernel(
    n,
    tokens_h,
    gain_h,
    wcv_h,
    wco_h,
    wci_h,
    taps_h,
    wq_h,
    wkv_h,
    wr_h,
    qg_h,
    kvg_h,
    wqn_h,
    wqr_h,
    wkn_h,
    wva_h,
    woc_h,
    woa_h,
    cos_h,
    sin_h,
    out_ref,
    tok,
    gain,
    wcv,
    wco,
    wci,
    taps,
    wq,
    wkv,
    wr,
    qg,
    kvg,
    wqn,
    wqr,
    wkn,
    wva,
    woc,
    woa,
    cosine,
    sine,
    xt,
    part,
    got,
    own,
    qp,
    kvp,
    kvr,
    gate,
    before,
    after,
    acc,
    put_near,
    got_near,
    put_far,
    got_far,
    load_sem,
    s_tok,
    r_tok,
    s_z,
    r_z,
    s_xf,
    r_xf,
    s_q,
    r_q,
    s_kv,
    r_kv,
    s_kz,
    r_kz,
    s_kf,
    r_kf,
    s_p,
    r_p,
    s_h,
    r_h,
    s_o,
    r_o,
):
    f32, bf16 = jnp.float32, jnp.bfloat16
    s, t = lax.axis_index("sp"), lax.axis_index("tp")
    core = lax.rem(t, 2)
    near = t + 1 - 2 * core
    far = lax.rem(t + 2, n)
    diag = lax.rem(near + 2, n)
    rows, width = tok.shape[1], tok.shape[2]
    cw = wcv.shape[1]
    tp_peers = (near, far, diag)

    loads = [
        (tokens_h, tok.at[t]),
        (gain_h, gain),
        (wq_h, wq),
        (wkv_h, wkv),
        (wr_h, wr),
        (wcv_h, wcv),
        (wco_h, wco),
        (wci_h, wci),
        (taps_h, taps),
        (qg_h, qg),
        (kvg_h, kvg),
        (wqn_h, wqn),
        (wqr_h, wqr),
        (wkn_h, wkn),
        (wva_h, wva),
        (cos_h.at[s], cosine),
        (sin_h.at[s], sine),
    ]
    for j in range(n):
        columns = pl.ds(j * width, width)
        loads.append((woa_h.at[:, columns], woa.at[j]))
        loads.append((woc_h.at[:, columns], woc.at[j]))
    loads = [pltpu.make_async_copy(a, b, load_sem.at[i]) for i, (a, b) in enumerate(loads)]
    for load in loads:
        load.start()

    barrier = pltpu.get_barrier_semaphore()
    for peer in tp_peers:
        pl.semaphore_signal(barrier, inc=1, device_id={"sp": s, "tp": peer}, device_id_type=MESH)
    for k in range(1, n):
        pl.semaphore_signal(
            barrier, inc=1, device_id={"sp": lax.rem(s + k, n), "tp": t}, device_id_type=MESH
        )
    loads[0].wait()
    pl.semaphore_wait(barrier, 2 * (n - 1))

    tok_far = copy_to(tok.at[t], tok.at[t], s_tok.at[0], r_tok.at[0], s, far)
    tok_near = copy_to(tok.at[t], tok.at[t], s_tok.at[1], r_tok.at[1], s, near)
    tok_fwd = copy_to(tok.at[far], tok.at[far], s_tok.at[2], r_tok.at[2], s, near)
    z_own = copy_to(tok.at[t], xt.at[s], s_z.at[0], r_z.at[s], t, t)
    z_far = copy_to(tok.at[far], xt.at[s], s_z.at[1], r_z.at[s], far, t)
    tok_far.start()

    @pl.when(t != s)
    def _():
        z_own.start()

    tok_near.start()
    for load in loads[1:]:
        load.wait()
    copy_to(tok.at[far], tok.at[far], s_tok.at[0], r_tok.at[0], s, far).wait_recv()
    tok_fwd.start()

    @pl.when(far != s)
    def _():
        z_far.start()

    copy_to(tok.at[near], tok.at[near], s_tok.at[1], r_tok.at[1], s, near).wait_recv()
    copy_to(tok.at[diag], tok.at[diag], s_tok.at[2], r_tok.at[2], s, near).wait_recv()

    squares = jnp.zeros((rows, 1), f32)
    q_sum = jnp.zeros((rows, wq.shape[2]), f32)
    kv_sum = jnp.zeros((rows, wkv.shape[0]), f32)
    r_sum = jnp.zeros((rows, wr.shape[0]), f32)
    for j in range(n):
        piece = tok[j].astype(f32)
        squares = squares + jnp.sum(piece * piece, axis=1, keepdims=True)
        scaled = (piece * gain[j * width : (j + 1) * width][None, :].astype(f32)).astype(bf16)
        kv_sum = kv_sum + dot_t(scaled, wkv[:, j * width : (j + 1) * width])
        r_sum = r_sum + dot_t(scaled, wr[:, j * width : (j + 1) * width])
        q_sum = q_sum + dot(scaled, wq[j])
    row_scale = lax.rsqrt(squares / (n * width) + EPS)
    kw = wkv.shape[0]
    place = (
        lax.broadcasted_iota(jnp.int32, (kw, 2 * kw), 1)
        == lax.broadcasted_iota(jnp.int32, (kw, 2 * kw), 0) + kw * core
    )
    place = jnp.where(place, 1.0, 0.0).astype(bf16)
    kvp[t] = dot((row_scale * kv_sum).astype(bf16), place).astype(bf16)
    kv_sends = [
        copy_to(kvp.at[t], kvp.at[t], s_kv.at[i], r_kv.at[i], s, p) for i, p in enumerate(tp_peers)
    ]
    for copy in (kv_sends[1], kv_sends[2], kv_sends[0]):
        copy.start()
    qp[t] = (row_scale * q_sum).astype(bf16)
    q_sends = [
        copy_to(qp.at[t], qp.at[t], s_q.at[i], r_q.at[i], s, p) for i, p in enumerate(tp_peers)
    ]
    for copy in (q_sends[1], q_sends[2], q_sends[0]):
        copy.start()

    meets = lax.rem(s, 2) == core
    my_gain = gain[pl.ds(pl.multiple_of(s * width, width), width)][None, :].astype(f32)
    p_sends = []

    def conv_part(block):
        scaled = (block.astype(f32) * my_gain).astype(bf16)
        return dot(scaled, wcv[...]), dot(scaled, wco[...]), dot(scaled, wci[...])

    upper = lax.div(s, n // 2)
    step = 1 - 2 * upper
    inner = s + upper * (n - 1 - 2 * s)

    def conv_block(i, mirrored, way, onward):
        z = mirrored + upper * (n - 1 - 2 * mirrored)
        fwd = copy_to(xt.at[z], xt.at[z], s_xf.at[i], r_xf.at[z], s, near)

        @pl.when(meets)
        def _():
            copy_to(xt.at[z], xt.at[z], s_z.at[0], r_z.at[z], z, t).wait_recv()
            fwd.start()

        @pl.when(jnp.logical_not(meets))
        def _():
            fwd.wait_recv()

        for m, product in enumerate(conv_part(xt[z])):
            copy = copy_to(
                part.at[i, m], got.at[way, z, m], s_p.at[i, m], r_p.at[way, z, m], onward, t
            )

            @pl.when(inner > 0)
            def _():
                copy.wait_recv()
                part[i, m] = (product + got[way, z, m].astype(f32)).astype(bf16)

            @pl.when(inner == 0)
            def _():
                part[i, m] = product.astype(bf16)

            copy.start()
            p_sends.append(copy)
        p_sends.append(fwd)

    conv_block(0, n - 1, upper, s + step)

    cos_v, sin_v = cosine[...], sine[...]
    lanes = cos_v.shape[1]
    turn_r = lax.broadcasted_iota(jnp.int32, (lanes, lanes), 0)
    turn_c = lax.broadcasted_iota(jnp.int32, (lanes, lanes), 1)
    half = ROPE // 2
    low = lax.rem(turn_c, ROPE) < half
    turn = jnp.where(
        low & (turn_r == turn_c + half), -1.0, jnp.where((~low) & (turn_r == turn_c - half), 1.0, 0.0)
    ).astype(bf16)
    spread_r = lax.broadcasted_iota(jnp.int32, (ROPE, lanes), 0)
    spread_c = lax.broadcasted_iota(jnp.int32, (ROPE, lanes), 1)
    spread = jnp.where(lax.rem(spread_c, ROPE) == spread_r, 1.0, 0.0).astype(bf16)
    rope_raw = dot((row_scale * r_sum).astype(bf16), spread).astype(bf16)
    k_rope = (rope_raw.astype(f32) * cos_v + dot(rope_raw, turn) * sin_v).astype(bf16)
    for i, p in enumerate(tp_peers):
        copy_to(kvp.at[p], kvp.at[p], s_kv.at[i], r_kv.at[i], s, p).wait_recv()
    kv_float = jnp.concatenate(
        [kvp[j].astype(f32) + kvp[j + 1].astype(f32) for j in range(0, n, 2)], axis=1
    )
    kv_scale = lax.rsqrt(jnp.mean(kv_float * kv_float, axis=1, keepdims=True) + EPS)
    lat = kv_float.shape[1]
    kvr[s, :, :lat] = (kv_float * kv_scale * kvg[...][None, :].astype(f32)).astype(bf16)
    kvr[s, :, lat:] = k_rope
    def quarter(index):
        return pl.ds(pl.multiple_of(index * (rows // n), rows // n), rows // n)

    mine = quarter(t)
    kz_sends = []
    for k in (2, 1, 3):
        z = lax.rem(s + k, n)
        copy = copy_to(
            kvr.at[s, mine], kvr.at[s, mine], s_kz.at[k - 1], r_kz.at[k - 1], z, t
        )
        copy.start()
        kz_sends.append(copy)

    conv_block(1, n - 2, upper, s + step)
    conv_block(2, 1 - inner, upper + inner * step, s + step * (1 - 2 * inner))
    for i, product in enumerate(conv_part(tok[s])):
        own[i] = product

    for i, p in enumerate(tp_peers):
        copy_to(qp.at[p], qp.at[p], s_q.at[i], r_q.at[i], s, p).wait_recv()
    q_float = [qp[j].astype(f32) for j in range(n)]
    qw = q_float[0].shape[1]
    q_square = sum(jnp.sum(q * q, axis=1, keepdims=True) for q in q_float)
    q_scale = lax.rsqrt(q_square / (n * qw) + EPS)
    q_normed = jnp.concatenate(
        [(q * q_scale * qg[j * qw : (j + 1) * qw][None, :].astype(f32)).astype(bf16) for j, q in enumerate(q_float)], axis=1
    )
    q_nope = dot(q_normed, wqn[...]).astype(bf16)
    q_raw = dot(q_normed, wqr[...])
    w_turned = dot(wqr[...], turn).astype(bf16)
    q_rope = (q_raw * cos_v + dot(q_normed, w_turned) * sin_v).astype(bf16)

    kf_sends = []
    for k in (2, 1, 3):
        z = lax.rem(s + n - k, n)
        copy_to(
            kvr.at[z, mine], kvr.at[z, mine], s_kz.at[k - 1], r_kz.at[k - 1], z, t
        ).wait_recv()
        for i, p in enumerate(tp_peers):
            copy = copy_to(
                kvr.at[z, mine], kvr.at[z, mine], s_kf.at[k - 1, i], r_kf.at[k - 1, i], s, p
            )
            copy.start()
            kf_sends.append(copy)
    for k in (2, 1, 3):
        z = lax.rem(s + n - k, n)
        for i, p in enumerate(tp_peers):
            rest = kvr.at[z, quarter(p)]
            copy_to(rest, rest, s_kf.at[k - 1, i], r_kf.at[k - 1, i], s, p).wait_recv()

    latent = jnp.concatenate([kvr[j, :, :lat] for j in range(n)], axis=0)
    ropes = jnp.concatenate([kvr[j, :, lat:] for j in range(n)], axis=0)
    keys = dot(latent, wkn[...]).astype(bf16)
    values = dot(latent, wva[...]).astype(bf16)
    heads = wqn.shape[1] // NOPE
    factor = (NOPE + ROPE) ** (-0.5)
    pair = 2 * NOPE
    lane = lax.broadcasted_iota(jnp.int32, (rows, pair), 1)
    lane_r = lax.broadcasted_iota(jnp.int32, (rows, lanes), 1)
    pieces = []
    for p in range(heads // 2):
        cut = slice(p * pair, (p + 1) * pair)
        key_pair = jnp.concatenate([keys[:, cut], ropes], axis=1)
        value_pair = values[:, cut]
        outs = []
        for i in range(2):
            h = 2 * p + i
            in_head = (lane >= i * NOPE) & (lane < (i + 1) * NOPE)
            in_rope = (lane_r >= h * ROPE) & (lane_r < (h + 1) * ROPE)
            query = jnp.concatenate(
                [
                    jnp.where(in_head, q_nope[:, cut].astype(f32), 0.0).astype(bf16),
                    jnp.where(in_rope, q_rope.astype(f32), 0.0).astype(bf16),
                ],
                axis=1,
            )
            scores = dot_t(query, key_pair) * factor
            peak = jnp.max(scores, axis=1, keepdims=True)
            weights = jnp.exp(scores - peak)
            total = jnp.sum(weights, axis=1, keepdims=True)
            outs.append(dot(weights.astype(bf16), value_pair) / total)
        pieces.append(jnp.where(lane < NOPE, outs[0], outs[1]).astype(bf16))
    y_attn = jnp.concatenate(pieces, axis=1)
    for j in range(n):
        acc[j] = dot(y_attn, woa[j])

    for way in (1 - upper, upper):

        @pl.when((way == 1 - upper) | (inner > 0))
        def _():
            for m in range(3):
                copy_to(
                    part.at[0, m], got.at[way, s, m], s_p.at[0, m], r_p.at[way, s, m], s, near
                ).wait_recv()
                own[m] = own[m] + got[way, s, m].astype(f32)

    def summed(i):
        return (row_scale * own[i]).astype(bf16).astype(f32)

    gated = (summed(2) * summed(0)).astype(bf16)
    gate[...] = gated
    edge = before.shape[0]
    up = copy_to(gate.at[pl.ds(rows - edge, edge)], before, s_h.at[0], r_h.at[0], s + 1, t)
    down = copy_to(gate.at[pl.ds(0, edge)], after, s_h.at[1], r_h.at[1], s - 1, t)

    @pl.when(s < n - 1)
    def _():
        up.start()

    @pl.when(s > 0)
    def _():
        down.start()

    conv_outer = summed(1)
    middle = gated.astype(f32)
    kernel = [taps[i : i + 1, :].astype(f32) for i in range(3)]
    row = lax.broadcasted_iota(jnp.int32, middle.shape, 0)
    previous = pltpu.roll(middle, 1, 0)
    following = pltpu.roll(middle, rows - 1, 0)

    @pl.when(s > 0)
    def _():
        up.wait_recv()

    @pl.when(s == 0)
    def _():
        before[...] = jnp.zeros_like(before)

    @pl.when(s < n - 1)
    def _():
        down.wait_recv()

    @pl.when(s == n - 1)
    def _():
        after[...] = jnp.zeros_like(after)

    first = before[...].astype(f32)[edge - 1 : edge, :]
    last = after[...].astype(f32)[0:1, :]
    previous = jnp.where(row == 0, first, previous)
    following = jnp.where(row == rows - 1, last, following)
    conv_out = previous * kernel[0] + middle * kernel[1] + following * kernel[2]
    y_conv = (conv_outer * conv_out).astype(bf16)

    def share(j):
        return acc[j] + dot(y_conv, woc[j])

    put_near[0] = share(diag).astype(bf16)
    o_diag = copy_to(put_near.at[0], got_near.at[0], s_o.at[0], r_o.at[0], s, near)
    o_diag.start()
    far_share = share(far).astype(bf16).astype(f32)
    o_diag.wait_recv()
    put_far[...] = (far_share + got_near[0].astype(f32)).astype(bf16)
    o_far = copy_to(put_far, got_far, s_o.at[1], r_o.at[1], s, far)
    o_far.start()
    put_near[1] = share(near).astype(bf16)
    o_near = copy_to(put_near.at[1], got_near.at[1], s_o.at[2], r_o.at[2], s, near)
    o_near.start()
    my_share = share(t).astype(bf16).astype(f32)
    o_near.wait_recv()
    my_share = my_share + got_near[1].astype(f32)

    tok_far.wait_send()
    tok_near.wait_send()
    tok_fwd.wait_send()

    @pl.when(t != s)
    def _():
        z_own.wait_send()

    @pl.when(far != s)
    def _():
        z_far.wait_send()

    for copy in kv_sends + q_sends + kz_sends + kf_sends:
        copy.wait_send()
    for i, copy in enumerate(p_sends):
        if i % 4 < 3:
            copy.wait_send()
        else:

            @pl.when(meets)
            def _():
                copy.wait_send()

    @pl.when(s < n - 1)
    def _():
        up.wait_send()

    @pl.when(s > 0)
    def _():
        down.wait_send()

    o_diag.wait_send()
    o_near.wait_send()
    o_far.wait()
    out_ref[...] = (my_share + got_far[...].astype(f32)).astype(bf16)


def fits(sp, tp, tokens, mix_gain, w_conv_value, *others):
    rows, width = tokens.shape
    return sp == tp == 4 and rows * sp <= width * tp and width % 128 == 0 and rows % 64 == 0


def fused(
    sp,
    tp,
    tokens,
    mix_gain,
    w_conv_value,
    w_conv_outer,
    w_conv_inner,
    conv_kernel,
    w_q_down,
    w_kv_down,
    w_rope_key,
    q_gain,
    kv_gain,
    w_q_nope,
    w_q_rope,
    w_k_nope,
    w_value,
    w_out_conv,
    w_out_attn,
):
    f32, bf16 = jnp.float32, jnp.bfloat16
    n = tp
    rows, width = tokens.shape
    heads = w_q_nope.shape[1] // NOPE
    inverse = np.float32(THETA) ** (-np.arange(0, ROPE, 2, dtype=np.float32) / np.float32(ROPE))
    phase = np.arange(sp * rows, dtype=np.float32)[:, None] * inverse[None, :].astype(np.float32)
    phase = np.tile(phase, (1, 2 * heads)).reshape(sp, rows, heads * ROPE)
    cosine, sine = np.cos(phase).astype(np.float32), np.sin(phase).astype(np.float32)
    operands = (
        tokens,
        mix_gain,
        w_conv_value,
        w_conv_outer,
        w_conv_inner,
        conv_kernel,
        w_q_down.reshape(n, width, -1),
        w_kv_down.T,
        w_rope_key.T,
        q_gain,
        kv_gain,
        w_q_nope,
        w_q_rope,
        w_k_nope,
        w_value,
        w_out_conv,
        w_out_attn,
        jnp.asarray(cosine),
        jnp.asarray(sine),
    )
    vm = pltpu.VMEM
    cw = w_conv_value.shape[1]
    lat = kv_gain.shape[0]
    lanes = heads * ROPE
    scratch = [vm((n, rows, width), bf16)]
    scratch += [vm(x.shape, x.dtype) for x in operands[1:15]]
    scratch += [vm((n, w_out_conv.shape[0], width), bf16)] * 2
    scratch += [vm((rows, lanes), f32)] * 2
    scratch += [
        vm((n, rows, width), bf16),
        vm((n - 1, 3, rows, cw), bf16),
        vm((2, n, 3, rows, cw), bf16),
        vm((3, rows, cw), f32),
        vm((n, rows, w_q_down.shape[1]), bf16),
        vm((n, rows, 2 * w_kv_down.shape[1]), bf16),
        vm((n, rows, lat + lanes), bf16),
        vm((rows, cw), bf16),
        vm((16, cw), bf16),
        vm((16, cw), bf16),
        vm((n, rows, width), f32),
        vm((2, rows, width), bf16),
        vm((2, rows, width), bf16),
        vm((rows, width), bf16),
        vm((rows, width), bf16),
    ]
    dma = pltpu.SemaphoreType.DMA
    scratch += [dma((17 + 2 * n,)), dma((3,)), dma((3,)), dma((2,)), dma((n,))]
    scratch += [dma((n - 1,)), dma((n,))]
    scratch += [dma((n - 1,))] * 6
    scratch += [dma((n - 1, n - 1))] * 2
    scratch += [dma((n - 1, 3)), dma((2, n, 3))]
    scratch += [dma((2,)), dma((2,)), dma((3,)), dma((3,))]
    return pl.pallas_call(
        functools.partial(mixer_kernel, n),
        out_shape=jax.ShapeDtypeStruct((rows, width), bf16),
        in_specs=[pl.BlockSpec(memory_space=pl.ANY)] * len(operands),
        out_specs=pl.BlockSpec(memory_space=pltpu.VMEM),
        scratch_shapes=scratch,
        compiler_params=pltpu.CompilerParams(collective_id=0, has_side_effects=True),
    )(*operands)


def solution(mesh):
    placed = (
        P(("grp", "sp"), "tp"),
        P(),
        P("sp", "tp"),
        P("sp", "tp"),
        P("sp", "tp"),
        P(None, "tp"),
        P(None, "tp"),
        P(None, "tp"),
        P(),
        P(),
        P(),
        P(None, "tp"),
        P(None, "tp"),
        P(None, "tp"),
        P(None, "tp"),
        P("tp", None),
        P("tp", None),
    )
    sp, tp = mesh.shape["sp"], mesh.shape["tp"]

    def per_device(*args):
        if fits(sp, tp, *args):
            return fused(sp, tp, *args)
        return gathered_weights(*args)

    return jax.shard_map(
        per_device, mesh=mesh, in_specs=placed, out_specs=P(("grp", "sp"), "tp"), check_vma=False
    )
```

profile of v0, /device:TPU:0, one launch (start us, length us, event | category | flops | bytes accessed | tf_op | source)
XLA Modules:
  0.0 46.2 jit_solution(15914504101240747189)
XLA Ops:
  0.0 44.6 %shard_map.181 = bf16[128,512]{1,0:T(8,128)(2,1)} custom-call(bf16[128,512]{1,0:T(8,128)(2,1)} %tokens_h.1, bf16[2048]{0:T(1024)(128)(2,1)} %gain_h.1, bf16[512,256]{1,0:T(8,128)(2,1)} %wcv_h.1, bf16[512,256]{1,0:T(8,128)(2,1)} %wco_h.1, bf16[512,256]{1,0:T(8,128)(2,1)} %wci_h.1, bf16[3,256]{1,0:T(4,128)(2,1)} %taps_h.1, bf16[4,512,128]{2,1,0:T(8,128)(2,1)} %bitcast.3, ...), custom_call_target="tpu_custom_call" | custom-call | tf_op jit(solution)/shard_map/pallas_call | solution.py:732
  44.6 1.6 %copy.21 = bf16[128,512]{1,0:T(8,128)(2,1)} copy(bf16[128,512]{1,0:T(8,128)(2,1)} %shard_map.181) | data formatting | bytes 262144
where the time goes:
time: 46.4 us; the launch traced here: 46.2 us
  Pallas kernels  44.6 us (96%)
  local copies, waits for them, and re-layouts  1.57 us (3%)
    pallas_call x1, Pallas kernels, fused(): pl.pallas_call(functools.partial(mixer_kernel, n), out_shape=jax.ShapeDty...  44.6 us
    unnamed x1, local copies, waits for them, and re-layouts  1.57 us

commit v1 on v0

--- a/solution.py
+++ b/solution.py
@@ -401,7 +401,9 @@
         def _():
             fwd.wait_recv()
 
-        for m, product in enumerate(conv_part(xt[z])):
+        products = conv_part(xt[z])
+        for m in (0, 2, 1):
+            product = products[m]
             copy = copy_to(
                 part.at[i, m], got.at[way, z, m], s_p.at[i, m], r_p.at[way, z, m], onward, t
             )
@@ -419,7 +421,8 @@
             p_sends.append(copy)
         p_sends.append(fwd)
 
-    conv_block(0, n - 1, upper, s + step)
+    for i, product in enumerate(conv_part(tok[s])):
+        own[i] = product
 
     cos_v, sin_v = cosine[...], sine[...]
     lanes = cos_v.shape[1]
@@ -457,10 +460,7 @@
         copy.start()
         kz_sends.append(copy)
 
-    conv_block(1, n - 2, upper, s + step)
-    conv_block(2, 1 - inner, upper + inner * step, s + step * (1 - 2 * inner))
-    for i, product in enumerate(conv_part(tok[s])):
-        own[i] = product
+    conv_block(0, n - 1, upper, s + step)
 
     for i, p in enumerate(tp_peers):
         copy_to(qp.at[p], qp.at[p], s_q.at[i], r_q.at[i], s, p).wait_recv()
@@ -476,6 +476,7 @@
     w_turned = dot(wqr[...], turn).astype(bf16)
     q_rope = (q_raw * cos_v + dot(q_normed, w_turned) * sin_v).astype(bf16)
 
+    conv_block(1, n - 2, upper, s + step)
     kf_sends = []
     for k in (2, 1, 3):
         z = lax.rem(s + n - k, n)
@@ -488,6 +489,7 @@
             )
             copy.start()
             kf_sends.append(copy)
+    conv_block(2, 1 - inner, upper + inner * step, s + step * (1 - 2 * inner))
     for k in (2, 1, 3):
         z = lax.rem(s + n - k, n)
         for i, p in enumerate(tp_peers):
@@ -530,15 +532,18 @@
     for j in range(n):
         acc[j] = dot(y_attn, woa[j])
 
-    for way in (1 - upper, upper):
-
-        @pl.when((way == 1 - upper) | (inner > 0))
-        def _():
-            for m in range(3):
+    def take(m):
+        for way in (1 - upper, upper):
+
+            @pl.when((way == 1 - upper) | (inner > 0))
+            def _():
                 copy_to(
                     part.at[0, m], got.at[way, s, m], s_p.at[0, m], r_p.at[way, s, m], s, near
                 ).wait_recv()
                 own[m] = own[m] + got[way, s, m].astype(f32)
+
+    take(0)
+    take(2)
 
     def summed(i):
         return (row_scale * own[i]).astype(bf16).astype(f32)
@@ -557,6 +562,7 @@
     def _():
         down.start()
 
+    take(1)
     conv_outer = summed(1)
     middle = gated.astype(f32)
     kernel = [taps[i : i + 1, :].astype(f32) for i in range(3)]

time: 46.4 us -> 45.1 us (0.972)
  Pallas kernels: 44.6 us -> 43.4 us
    pallas_call x1, Pallas kernels: 44.6 us -> 43.4 us  [fused(): pl.pallas_call(functools.partial(mixer_kernel, n), out_shape=jax.ShapeDty...]
where the time goes in v1:
time: 45.1 us; the launch traced here: 44.9 us
  Pallas kernels  43.4 us (96%)
  local copies, waits for them, and re-layouts  1.57 us (3%)
    pallas_call x1, Pallas kernels, fused(): pl.pallas_call(functools.partial(mixer_kernel, n), out_shape=jax.ShapeDty...  43.4 us
    unnamed x1, local copies, waits for them, and re-layouts  1.57 us

profile of v1, /device:TPU:0, one launch (start us, length us, event | category | flops | bytes accessed | tf_op | source)
XLA Modules:
  0.0 44.9 jit_solution(1375635542248511643)
XLA Ops:
  0.0 43.4 %shard_map.181 = bf16[128,512]{1,0:T(8,128)(2,1)} custom-call(bf16[128,512]{1,0:T(8,128)(2,1)} %tokens_h.1, bf16[2048]{0:T(1024)(128)(2,1)} %gain_h.1, bf16[512,256]{1,0:T(8,128)(2,1)} %wcv_h.1, bf16[512,256]{1,0:T(8,128)(2,1)} %wco_h.1, bf16[512,256]{1,0:T(8,128)(2,1)} %wci_h.1, bf16[3,256]{1,0:T(4,128)(2,1)} %taps_h.1, bf16[4,512,128]{2,1,0:T(8,128)(2,1)} %bitcast.3, ...), custom_call_target="tpu_custom_call" | custom-call | tf_op jit(solution)/shard_map/pallas_call | solution.py:738
  43.4 1.6 %copy.21 = bf16[128,512]{1,0:T(8,128)(2,1)} copy(bf16[128,512]{1,0:T(8,128)(2,1)} %shard_map.181) | data formatting | bytes 262144

commit v2 on v1

--- a/solution.py
+++ b/solution.py
@@ -177,13 +177,13 @@
     )
 
 
-def copy_to(src, dst, send, recv, sp, tp):
+def copy_to(src, dst, send, recv, sp, tp, **group):
     return pltpu.make_async_remote_copy(
         src_ref=src,
         dst_ref=dst,
         send_sem=send,
         recv_sem=recv,
-        device_id={"sp": sp, "tp": tp},
+        device_id={"sp": sp, "tp": tp, **group},
         device_id_type=MESH,
     )
 
@@ -237,6 +237,7 @@
     woa,
     cosine,
     sine,
+    wx,
     xt,
     part,
     got,
@@ -259,6 +260,10 @@
     r_z,
     s_xf,
     r_xf,
+    s_w,
+    r_w,
+    s_y,
+    r_y,
     s_q,
     r_q,
     s_kv,
@@ -275,7 +280,7 @@
     r_o,
 ):
     f32, bf16 = jnp.float32, jnp.bfloat16
-    s, t = lax.axis_index("sp"), lax.axis_index("tp")
+    g, s, t = lax.axis_index("grp"), lax.axis_index("sp"), lax.axis_index("tp")
     core = lax.rem(t, 2)
     near = t + 1 - 2 * core
     far = lax.rem(t + 2, n)
@@ -283,6 +288,12 @@
     rows, width = tok.shape[1], tok.shape[2]
     cw = wcv.shape[1]
     tp_peers = (near, far, diag)
+    upper = lax.div(s, n // 2)
+    side = lax.div(t, 2)
+    is_hub = (s == 1) | (s == n - 2)
+    mate = s + 1 - 2 * lax.rem(s, 2)
+    hub_over = n // 2 - upper
+    end_over = (n - 1) * (1 - upper)
 
     loads = [
         (tokens_h, tok.at[t]),
@@ -318,30 +329,69 @@
         pl.semaphore_signal(
             barrier, inc=1, device_id={"sp": lax.rem(s + k, n), "tp": t}, device_id_type=MESH
         )
+    pl.semaphore_signal(
+        barrier, inc=1, device_id={"grp": 1 - g, "sp": s, "tp": t}, device_id_type=MESH
+    )
     loads[0].wait()
-    pl.semaphore_wait(barrier, 2 * (n - 1))
+    pl.semaphore_wait(barrier, 2 * (n - 1) + 1)
 
     tok_far = copy_to(tok.at[t], tok.at[t], s_tok.at[0], r_tok.at[0], s, far)
     tok_near = copy_to(tok.at[t], tok.at[t], s_tok.at[1], r_tok.at[1], s, near)
     tok_fwd = copy_to(tok.at[far], tok.at[far], s_tok.at[2], r_tok.at[2], s, near)
-    z_own = copy_to(tok.at[t], xt.at[s], s_z.at[0], r_z.at[s], t, t)
-    z_far = copy_to(tok.at[far], xt.at[s], s_z.at[1], r_z.at[s], far, t)
+    z_slot = xt.at[jnp.where(is_hub, 1, 0), core]
+    z_recv = r_z.at[jnp.where(is_hub, 1, 0)]
+    z_own = copy_to(tok.at[t], z_slot, s_z, z_recv, hub_over, t)
+    z_far = copy_to(tok.at[far], z_slot, s_z, z_recv, hub_over, t)
+    own_first = side != upper
     tok_far.start()
 
-    @pl.when(t != s)
+    @pl.when(own_first)
     def _():
         z_own.start()
 
     tok_near.start()
-    for load in loads[1:]:
+    weights = (wcv, wco, wci)
+    order = (2, 0, 1)
+    chunk = wcv.shape[0] // 4
+    chunks = [(m, c) for m in order for c in range(2)]
+
+    def chunk_rows(half, c):
+        return pl.ds(pl.multiple_of((2 * half + c) * chunk, chunk), chunk)
+
+    w_sends, y_sends = [], []
+    for k, (m, c) in enumerate(chunks):
+        w_sends.append(
+            copy_to(
+                weights[m].at[chunk_rows(g, c)],
+                wx.at[m, chunk_rows(g, c)],
+                s_w.at[k],
+                r_w.at[k],
+                mate,
+                t,
+            )
+        )
+        block = wx.at[m, chunk_rows(g, c)]
+        y_sends.append(copy_to(block, block, s_y.at[k], r_y.at[k], s, t, grp=1 - g))
+
+    def relay(k):
+        w_sends[k].wait_recv()
+        y_sends[k].start()
+
+    for load in loads[5:8]:
+        load.wait()
+    for copy in w_sends[:3]:
+        copy.start()
+    for load in loads[1:5] + loads[8:]:
         load.wait()
     copy_to(tok.at[far], tok.at[far], s_tok.at[0], r_tok.at[0], s, far).wait_recv()
     tok_fwd.start()
 
-    @pl.when(far != s)
+    @pl.when(jnp.logical_not(own_first))
     def _():
         z_far.start()
 
+    for copy in w_sends[3:]:
+        copy.start()
     copy_to(tok.at[near], tok.at[near], s_tok.at[1], r_tok.at[1], s, near).wait_recv()
     copy_to(tok.at[diag], tok.at[diag], s_tok.at[2], r_tok.at[2], s, near).wait_recv()
 
@@ -376,53 +426,45 @@
     for copy in (q_sends[1], q_sends[2], q_sends[0]):
         copy.start()
 
-    meets = lax.rem(s, 2) == core
-    my_gain = gain[pl.ds(pl.multiple_of(s * width, width), width)][None, :].astype(f32)
+    def scaled_slice(block, f):
+        gain_f = gain[pl.ds(pl.multiple_of(f * width, width), width)][None, :].astype(f32)
+        return (block.astype(f32) * gain_f).astype(bf16)
+
+    mine_scaled = scaled_slice(tok[s], s)
+    for m in order:
+        own[m] = dot(mine_scaled, weights[m][...])
+    for k in range(3):
+        relay(k)
+
     p_sends = []
-
-    def conv_part(block):
-        scaled = (block.astype(f32) * my_gain).astype(bf16)
-        return dot(scaled, wcv[...]), dot(scaled, wco[...]), dot(scaled, wci[...])
-
-    upper = lax.div(s, n // 2)
-    step = 1 - 2 * upper
-    inner = s + upper * (n - 1 - 2 * s)
-
-    def conv_block(i, mirrored, way, onward):
-        z = mirrored + upper * (n - 1 - 2 * mirrored)
-        fwd = copy_to(xt.at[z], xt.at[z], s_xf.at[i], r_xf.at[z], s, near)
-
-        @pl.when(meets)
+    for i in range(2):
+        for m in range(3):
+            target = hub_over if i else end_over
+            p_sends.append(
+                copy_to(part.at[i, m], got.at[m], s_p.at[i, m], r_p.at[m], target, t)
+            )
+    x_sends = []
+    for i in range(2):
+        slot = xt.at[i, core]
+        x_sends.append(copy_to(slot, slot, s_xf.at[i], r_xf.at[i], s, near))
+
+    def conv_block(j):
+        m = order[j]
+        for k in (2 * j, 2 * j + 1):
+            y_sends[k].wait_recv()
+
+        @pl.when(is_hub)
         def _():
-            copy_to(xt.at[z], xt.at[z], s_z.at[0], r_z.at[z], z, t).wait_recv()
-            fwd.start()
-
-        @pl.when(jnp.logical_not(meets))
-        def _():
-            fwd.wait_recv()
-
-        products = conv_part(xt[z])
-        for m in (0, 2, 1):
-            product = products[m]
-            copy = copy_to(
-                part.at[i, m], got.at[way, z, m], s_p.at[i, m], r_p.at[way, z, m], onward, t
+            first = jnp.concatenate([xt[i, lax.rem(s, 2)] for i in range(2)], axis=0)
+            second = jnp.concatenate([xt[i, lax.rem(mate, 2)] for i in range(2)], axis=0)
+            total = dot(scaled_slice(first, s), weights[m][...]) + dot(
+                scaled_slice(second, mate), wx[m]
             )
-
-            @pl.when(inner > 0)
-            def _():
-                copy.wait_recv()
-                part[i, m] = (product + got[way, z, m].astype(f32)).astype(bf16)
-
-            @pl.when(inner == 0)
-            def _():
-                part[i, m] = product.astype(bf16)
-
-            copy.start()
-            p_sends.append(copy)
-        p_sends.append(fwd)
-
-    for i, product in enumerate(conv_part(tok[s])):
-        own[i] = product
+            for i in range(2):
+                part[i, m] = total[i * rows : (i + 1) * rows].astype(bf16)
+                p_sends[3 * i + m].start()
+
+        own[m] = own[m] + dot(scaled_slice(tok[mate], mate), wx[m])
 
     cos_v, sin_v = cosine[...], sine[...]
     lanes = cos_v.shape[1]
@@ -460,7 +502,19 @@
         copy.start()
         kz_sends.append(copy)
 
-    conv_block(0, n - 1, upper, s + step)
+    for k in range(3, 6):
+        relay(k)
+
+    @pl.when(is_hub)
+    def _():
+        for i in range(2):
+            slot = xt.at[i, core]
+            copy_to(slot, slot, s_z, r_z.at[i], s, near).wait_recv()
+            x_sends[i].start()
+        for copy in x_sends:
+            copy.wait_recv()
+
+    conv_block(0)
 
     for i, p in enumerate(tp_peers):
         copy_to(qp.at[p], qp.at[p], s_q.at[i], r_q.at[i], s, p).wait_recv()
@@ -476,7 +530,6 @@
     w_turned = dot(wqr[...], turn).astype(bf16)
     q_rope = (q_raw * cos_v + dot(q_normed, w_turned) * sin_v).astype(bf16)
 
-    conv_block(1, n - 2, upper, s + step)
     kf_sends = []
     for k in (2, 1, 3):
         z = lax.rem(s + n - k, n)
@@ -489,7 +542,8 @@
             )
             copy.start()
             kf_sends.append(copy)
-    conv_block(2, 1 - inner, upper + inner * step, s + step * (1 - 2 * inner))
+    conv_block(1)
+    conv_block(2)
     for k in (2, 1, 3):
         z = lax.rem(s + n - k, n)
         for i, p in enumerate(tp_peers):
@@ -533,17 +587,11 @@
         acc[j] = dot(y_attn, woa[j])
 
     def take(m):
-        for way in (1 - upper, upper):
-
-            @pl.when((way == 1 - upper) | (inner > 0))
-            def _():
-                copy_to(
-                    part.at[0, m], got.at[way, s, m], s_p.at[0, m], r_p.at[way, s, m], s, near
-                ).wait_recv()
-                own[m] = own[m] + got[way, s, m].astype(f32)
-
+        copy_to(part.at[0, m], got.at[m], s_p.at[0, m], r_p.at[m], s, near).wait_recv()
+        own[m] = own[m] + got[m].astype(f32)
+
+    take(2)
     take(0)
-    take(2)
 
     def summed(i):
         return (row_scale * own[i]).astype(bf16).astype(f32)
@@ -615,24 +663,14 @@
     tok_near.wait_send()
     tok_fwd.wait_send()
 
-    @pl.when(t != s)
-    def _():
-        z_own.wait_send()
-
-    @pl.when(far != s)
-    def _():
-        z_far.wait_send()
-
-    for copy in kv_sends + q_sends + kz_sends + kf_sends:
+    z_own.wait_send()
+    for copy in kv_sends + q_sends + kz_sends + kf_sends + w_sends + y_sends:
         copy.wait_send()
-    for i, copy in enumerate(p_sends):
-        if i % 4 < 3:
+
+    @pl.when(is_hub)
+    def _():
+        for copy in p_sends + x_sends:
             copy.wait_send()
-        else:
-
-            @pl.when(meets)
-            def _():
-                copy.wait_send()
 
     @pl.when(s < n - 1)
     def _():
@@ -648,9 +686,11 @@
     out_ref[...] = (my_share + got_far[...].astype(f32)).astype(bf16)
 
 
-def fits(sp, tp, tokens, mix_gain, w_conv_value, *others):
+def fits(grp, sp, tp, tokens, mix_gain, w_conv_value, *others):
     rows, width = tokens.shape
-    return sp == tp == 4 and rows * sp <= width * tp and width % 128 == 0 and rows % 64 == 0
+    if grp != 2 or sp != 4 or tp != 4 or rows * sp > width * tp:
+        return False
+    return width % 128 == 0 and rows % 64 == 0 and w_conv_value.shape[0] % 64 == 0
 
 
 def fused(
@@ -712,9 +752,10 @@
     scratch += [vm((n, w_out_conv.shape[0], width), bf16)] * 2
     scratch += [vm((rows, lanes), f32)] * 2
     scratch += [
-        vm((n, rows, width), bf16),
-        vm((n - 1, 3, rows, cw), bf16),
-        vm((2, n, 3, rows, cw), bf16),
+        vm((3,) + w_conv_value.shape, bf16),
+        vm((2, 2, rows, width), bf16),
+        vm((2, 3, rows, cw), bf16),
+        vm((3, rows, cw), bf16),
         vm((3, rows, cw), f32),
         vm((n, rows, w_q_down.shape[1]), bf16),
         vm((n, rows, 2 * w_kv_down.shape[1]), bf16),
@@ -729,11 +770,12 @@
         vm((rows, width), bf16),
     ]
     dma = pltpu.SemaphoreType.DMA
-    scratch += [dma((17 + 2 * n,)), dma((3,)), dma((3,)), dma((2,)), dma((n,))]
-    scratch += [dma((n - 1,)), dma((n,))]
+    scratch += [dma((17 + 2 * n,)), dma((3,)), dma((3,)), dma, dma((2,))]
+    scratch += [dma((2,))] * 2
+    scratch += [dma((6,))] * 4
     scratch += [dma((n - 1,))] * 6
     scratch += [dma((n - 1, n - 1))] * 2
-    scratch += [dma((n - 1, 3)), dma((2, n, 3))]
+    scratch += [dma((2, 3)), dma((3,))]
     scratch += [dma((2,)), dma((2,)), dma((3,)), dma((3,))]
     return pl.pallas_call(
         functools.partial(mixer_kernel, n),
@@ -765,10 +807,10 @@
         P("tp", None),
         P("tp", None),
     )
-    sp, tp = mesh.shape["sp"], mesh.shape["tp"]
+    grp, sp, tp = mesh.shape["grp"], mesh.shape["sp"], mesh.shape["tp"]
 
     def per_device(*args):
-        if fits(sp, tp, *args):
+        if fits(grp, sp, tp, *args):
             return fused(sp, tp, *args)
         return gathered_weights(*args)
 

time: 45.1 us -> 39.7 us (0.88)
  Pallas kernels: 43.4 us -> 37.9 us
    pallas_call x1, Pallas kernels: 43.4 us -> 37.9 us  [fused(): pl.pallas_call(functools.partial(mixer_kernel, n), out_shape=jax.ShapeDty...]
where the time goes in v2:
time: 39.7 us; the launch traced here: 39.5 us
  Pallas kernels  37.9 us (95%)
  local copies, waits for them, and re-layouts  1.57 us (4%)
    pallas_call x1, Pallas kernels, fused(): pl.pallas_call(functools.partial(mixer_kernel, n), out_shape=jax.ShapeDty...  37.9 us
    unnamed x1, local copies, waits for them, and re-layouts  1.57 us

profile of v2, /device:TPU:0, one launch (start us, length us, event | category | flops | bytes accessed | tf_op | source)
XLA Modules:
  0.0 39.5 jit_solution(9064360847704418163)
XLA Ops:
  0.0 37.9 %shard_map.181 = bf16[128,512]{1,0:T(8,128)(2,1)} custom-call(bf16[128,512]{1,0:T(8,128)(2,1)} %tokens_h.1, bf16[2048]{0:T(1024)(128)(2,1)} %gain_h.1, bf16[512,256]{1,0:T(8,128)(2,1)} %wcv_h.1, bf16[512,256]{1,0:T(8,128)(2,1)} %wco_h.1, bf16[512,256]{1,0:T(8,128)(2,1)} %wci_h.1, bf16[3,256]{1,0:T(4,128)(2,1)} %taps_h.1, bf16[4,512,128]{2,1,0:T(8,128)(2,1)} %bitcast.3, ...), custom_call_target="tpu_custom_call" | custom-call | tf_op jit(solution)/shard_map/pallas_call | solution.py:780
  37.9 1.6 %copy.21 = bf16[128,512]{1,0:T(8,128)(2,1)} copy(bf16[128,512]{1,0:T(8,128)(2,1)} %shard_map.181) | data formatting | bytes 262144

commit v3 on v2

--- a/solution.py
+++ b/solution.py
@@ -344,19 +344,15 @@
     z_far = copy_to(tok.at[far], z_slot, s_z, z_recv, hub_over, t)
     own_first = side != upper
     tok_far.start()
-
-    @pl.when(own_first)
-    def _():
-        z_own.start()
-
     tok_near.start()
     weights = (wcv, wco, wci)
     order = (2, 0, 1)
-    chunk = wcv.shape[0] // 4
-    chunks = [(m, c) for m in order for c in range(2)]
+    pieces_per = 4
+    chunk = wcv.shape[0] // (2 * pieces_per)
+    chunks = [(m, c) for m in order for c in range(pieces_per)]
 
     def chunk_rows(half, c):
-        return pl.ds(pl.multiple_of((2 * half + c) * chunk, chunk), chunk)
+        return pl.ds(pl.multiple_of((pieces_per * half + c) * chunk, chunk), chunk)
 
     w_sends, y_sends = [], []
     for k, (m, c) in enumerate(chunks):
@@ -379,7 +375,14 @@
 
     for load in loads[5:8]:
         load.wait()
-    for copy in w_sends[:3]:
+    for copy in w_sends[:4]:
+        copy.start()
+
+    @pl.when(own_first)
+    def _():
+        z_own.start()
+
+    for copy in w_sends[4:6]:
         copy.start()
     for load in loads[1:5] + loads[8:]:
         load.wait()
@@ -390,7 +393,7 @@
     def _():
         z_far.start()
 
-    for copy in w_sends[3:]:
+    for copy in w_sends[6:]:
         copy.start()
     copy_to(tok.at[near], tok.at[near], s_tok.at[1], r_tok.at[1], s, near).wait_recv()
     copy_to(tok.at[diag], tok.at[diag], s_tok.at[2], r_tok.at[2], s, near).wait_recv()
@@ -433,7 +436,7 @@
     mine_scaled = scaled_slice(tok[s], s)
     for m in order:
         own[m] = dot(mine_scaled, weights[m][...])
-    for k in range(3):
+    for k in range(4):
         relay(k)
 
     p_sends = []
@@ -450,7 +453,7 @@
 
     def conv_block(j):
         m = order[j]
-        for k in (2 * j, 2 * j + 1):
+        for k in range(pieces_per * j, pieces_per * (j + 1)):
             y_sends[k].wait_recv()
 
         @pl.when(is_hub)
@@ -502,7 +505,7 @@
         copy.start()
         kz_sends.append(copy)
 
-    for k in range(3, 6):
+    for k in range(4, 7):
         relay(k)
 
     @pl.when(is_hub)
@@ -515,6 +518,8 @@
             copy.wait_recv()
 
     conv_block(0)
+    for k in range(7, 10):
+        relay(k)
 
     for i, p in enumerate(tp_peers):
         copy_to(qp.at[p], qp.at[p], s_q.at[i], r_q.at[i], s, p).wait_recv()
@@ -530,6 +535,8 @@
     w_turned = dot(wqr[...], turn).astype(bf16)
     q_rope = (q_raw * cos_v + dot(q_normed, w_turned) * sin_v).astype(bf16)
 
+    for k in range(10, 12):
+        relay(k)
     kf_sends = []
     for k in (2, 1, 3):
         z = lax.rem(s + n - k, n)
@@ -772,14 +779,14 @@
     dma = pltpu.SemaphoreType.DMA
     scratch += [dma((17 + 2 * n,)), dma((3,)), dma((3,)), dma, dma((2,))]
     scratch += [dma((2,))] * 2
-    scratch += [dma((6,))] * 4
+    scratch += [dma((12,))] * 4
     scratch += [dma((n - 1,))] * 6
     scratch += [dma((n - 1, n - 1))] * 2
     scratch += [dma((2, 3)), dma((3,))]
     scratch += [dma((2,)), dma((2,)), dma((3,)), dma((3,))]
     return pl.pallas_call(
         functools.partial(mixer_kernel, n),
-        out_shape=jax.ShapeDtypeStruct((rows, width), bf16),
+        out_shape=pltpu.VMEM((rows, width), bf16),
         in_specs=[pl.BlockSpec(memory_space=pl.ANY)] * len(operands),
         out_specs=pl.BlockSpec(memory_space=pltpu.VMEM),
         scratch_shapes=scratch,

time: 39.7 us -> 35.9 us (0.904)
  Pallas kernels: 37.9 us -> 35.1 us
  local copies, waits for them, and re-layouts: 1.57 us -> 0.66 us
    pallas_call x1, Pallas kernels: 37.9 us -> 35.1 us  [fused(): pl.pallas_call(functools.partial(mixer_kernel, n), out_shape=pltpu.VMEM((...]
    unnamed x1, local copies, waits for them, and re-layouts: 1.57 us -> 0.66 us
where the time goes in v3:
time: 35.9 us; the launch traced here: 35.8 us
  Pallas kernels  35.1 us (98%)
  local copies, waits for them, and re-layouts  0.66 us (2%)
    pallas_call x1, Pallas kernels, fused(): pl.pallas_call(functools.partial(mixer_kernel, n), out_shape=pltpu.VMEM((...  35.1 us

profile of v3, /device:TPU:0, one launch (start us, length us, event | category | flops | bytes accessed | tf_op | source)
XLA Modules:
  0.0 35.8 jit_solution(5489234351166660882)
XLA Ops:
  0.0 35.1 %shard_map.181 = bf16[128,512]{1,0:T(8,128)(2,1)S(1)} custom-call(bf16[128,512]{1,0:T(8,128)(2,1)} %tokens_h.1, bf16[2048]{0:T(1024)(128)(2,1)} %gain_h.1, bf16[512,256]{1,0:T(8,128)(2,1)} %wcv_h.1, bf16[512,256]{1,0:T(8,128)(2,1)} %wco_h.1, bf16[512,256]{1,0:T(8,128)(2,1)} %wci_h.1, bf16[3,256]{1,0:T(4,128)(2,1)} %taps_h.1, bf16[4,512,128]{2,1,0:T(8,128)(2,1)} %bitcast.3, ...), custom_call_target="tpu_custom_call" | custom-call | tf_op jit(solution)/shard_map/pallas_call | solution.py:787
  35.1 0.7 %copy.21 = bf16[128,512]{1,0:T(8,128)(2,1)} copy(bf16[128,512]{1,0:T(8,128)(2,1)S(1)} %shard_map.181) | data formatting | bytes 262144

commit v4 on v3

--- a/solution.py
+++ b/solution.py
@@ -254,29 +254,18 @@
     put_far,
     got_far,
     load_sem,
-    s_tok,
+    sent,
     r_tok,
-    s_z,
     r_z,
-    s_xf,
     r_xf,
-    s_w,
     r_w,
-    s_y,
     r_y,
-    s_q,
     r_q,
-    s_kv,
     r_kv,
-    s_kz,
     r_kz,
-    s_kf,
     r_kf,
-    s_p,
     r_p,
-    s_h,
     r_h,
-    s_o,
     r_o,
 ):
     f32, bf16 = jnp.float32, jnp.bfloat16
@@ -318,7 +307,8 @@
         columns = pl.ds(j * width, width)
         loads.append((woa_h.at[:, columns], woa.at[j]))
         loads.append((woc_h.at[:, columns], woc.at[j]))
-    loads = [pltpu.make_async_copy(a, b, load_sem.at[i]) for i, (a, b) in enumerate(loads)]
+    groups = [0] + [2] * 4 + [1] * 3 + [3] * (len(loads) - 8)
+    loads = [pltpu.make_async_copy(a, b, load_sem.at[i]) for (a, b), i in zip(loads, groups)]
     for load in loads:
         load.start()
 
@@ -335,13 +325,13 @@
     loads[0].wait()
     pl.semaphore_wait(barrier, 2 * (n - 1) + 1)
 
-    tok_far = copy_to(tok.at[t], tok.at[t], s_tok.at[0], r_tok.at[0], s, far)
-    tok_near = copy_to(tok.at[t], tok.at[t], s_tok.at[1], r_tok.at[1], s, near)
-    tok_fwd = copy_to(tok.at[far], tok.at[far], s_tok.at[2], r_tok.at[2], s, near)
+    tok_far = copy_to(tok.at[t], tok.at[t], sent, r_tok.at[0], s, far)
+    tok_near = copy_to(tok.at[t], tok.at[t], sent, r_tok.at[1], s, near)
+    tok_fwd = copy_to(tok.at[far], tok.at[far], sent, r_tok.at[2], s, near)
     z_slot = xt.at[jnp.where(is_hub, 1, 0), core]
     z_recv = r_z.at[jnp.where(is_hub, 1, 0)]
-    z_own = copy_to(tok.at[t], z_slot, s_z, z_recv, hub_over, t)
-    z_far = copy_to(tok.at[far], z_slot, s_z, z_recv, hub_over, t)
+    z_own = copy_to(tok.at[t], z_slot, sent, z_recv, hub_over, t)
+    z_far = copy_to(tok.at[far], z_slot, sent, z_recv, hub_over, t)
     own_first = side != upper
     tok_far.start()
     tok_near.start()
@@ -360,14 +350,17 @@
             copy_to(
                 weights[m].at[chunk_rows(g, c)],
                 wx.at[m, chunk_rows(g, c)],
-                s_w.at[k],
+                sent,
                 r_w.at[k],
                 mate,
                 t,
             )
         )
         block = wx.at[m, chunk_rows(g, c)]
-        y_sends.append(copy_to(block, block, s_y.at[k], r_y.at[k], s, t, grp=1 - g))
+        y_sends.append(copy_to(block, block, sent, r_y.at[m], s, t, grp=1 - g))
+
+    def arrived(ref, sem):
+        copy_to(ref, ref, sent, sem, s, near).wait_recv()
 
     def relay(k):
         w_sends[k].wait_recv()
@@ -386,7 +379,7 @@
         copy.start()
     for load in loads[1:5] + loads[8:]:
         load.wait()
-    copy_to(tok.at[far], tok.at[far], s_tok.at[0], r_tok.at[0], s, far).wait_recv()
+    copy_to(tok.at[far], tok.at[far], sent, r_tok.at[0], s, far).wait_recv()
     tok_fwd.start()
 
     @pl.when(jnp.logical_not(own_first))
@@ -395,8 +388,8 @@
 
     for copy in w_sends[6:]:
         copy.start()
-    copy_to(tok.at[near], tok.at[near], s_tok.at[1], r_tok.at[1], s, near).wait_recv()
-    copy_to(tok.at[diag], tok.at[diag], s_tok.at[2], r_tok.at[2], s, near).wait_recv()
+    copy_to(tok.at[near], tok.at[near], sent, r_tok.at[1], s, near).wait_recv()
+    copy_to(tok.at[diag], tok.at[diag], sent, r_tok.at[2], s, near).wait_recv()
 
     squares = jnp.zeros((rows, 1), f32)
     q_sum = jnp.zeros((rows, wq.shape[2]), f32)
@@ -418,13 +411,13 @@
     place = jnp.where(place, 1.0, 0.0).astype(bf16)
     kvp[t] = dot((row_scale * kv_sum).astype(bf16), place).astype(bf16)
     kv_sends = [
-        copy_to(kvp.at[t], kvp.at[t], s_kv.at[i], r_kv.at[i], s, p) for i, p in enumerate(tp_peers)
+        copy_to(kvp.at[t], kvp.at[t], sent, r_kv, s, p) for i, p in enumerate(tp_peers)
     ]
     for copy in (kv_sends[1], kv_sends[2], kv_sends[0]):
         copy.start()
     qp[t] = (row_scale * q_sum).astype(bf16)
     q_sends = [
-        copy_to(qp.at[t], qp.at[t], s_q.at[i], r_q.at[i], s, p) for i, p in enumerate(tp_peers)
+        copy_to(qp.at[t], qp.at[t], sent, r_q, s, p) for i, p in enumerate(tp_peers)
     ]
     for copy in (q_sends[1], q_sends[2], q_sends[0]):
         copy.start()
@@ -439,22 +432,45 @@
     for k in range(4):
         relay(k)
 
+    edge = before.shape[0]
+    up = copy_to(gate.at[pl.ds(rows - edge, edge)], before, sent, r_h.at[0], s + 1, t)
+    down = copy_to(gate.at[pl.ds(0, edge)], after, sent, r_h.at[1], s - 1, t)
+
+    def take(m):
+        arrived(got.at[m], r_p.at[m])
+        own[m] = own[m] + got[m].astype(f32)
+
+    def summed(i):
+        return (row_scale * own[i]).astype(bf16).astype(f32)
+
+    def gate_part():
+        take(2)
+        take(0)
+        gate[...] = (summed(2) * summed(0)).astype(bf16)
+
+        @pl.when(s < n - 1)
+        def _():
+            up.start()
+
+        @pl.when(s > 0)
+        def _():
+            down.start()
+
     p_sends = []
     for i in range(2):
         for m in range(3):
             target = hub_over if i else end_over
             p_sends.append(
-                copy_to(part.at[i, m], got.at[m], s_p.at[i, m], r_p.at[m], target, t)
+                copy_to(part.at[i, m], got.at[m], sent, r_p.at[m], target, t)
             )
     x_sends = []
     for i in range(2):
         slot = xt.at[i, core]
-        x_sends.append(copy_to(slot, slot, s_xf.at[i], r_xf.at[i], s, near))
+        x_sends.append(copy_to(slot, slot, sent, r_xf, s, near))
 
     def conv_block(j):
         m = order[j]
-        for k in range(pieces_per * j, pieces_per * (j + 1)):
-            y_sends[k].wait_recv()
+        arrived(wx.at[m, pl.ds(0, wx.shape[1] // 2)], r_y.at[m])
 
         @pl.when(is_hub)
         def _():
@@ -483,8 +499,7 @@
     spread = jnp.where(lax.rem(spread_c, ROPE) == spread_r, 1.0, 0.0).astype(bf16)
     rope_raw = dot((row_scale * r_sum).astype(bf16), spread).astype(bf16)
     k_rope = (rope_raw.astype(f32) * cos_v + dot(rope_raw, turn) * sin_v).astype(bf16)
-    for i, p in enumerate(tp_peers):
-        copy_to(kvp.at[p], kvp.at[p], s_kv.at[i], r_kv.at[i], s, p).wait_recv()
+    arrived(kvp.at[pl.ds(0, n - 1)], r_kv)
     kv_float = jnp.concatenate(
         [kvp[j].astype(f32) + kvp[j + 1].astype(f32) for j in range(0, n, 2)], axis=1
     )
@@ -500,7 +515,7 @@
     for k in (2, 1, 3):
         z = lax.rem(s + k, n)
         copy = copy_to(
-            kvr.at[s, mine], kvr.at[s, mine], s_kz.at[k - 1], r_kz.at[k - 1], z, t
+            kvr.at[s, mine], kvr.at[s, mine], sent, r_kz.at[k - 1], z, t
         )
         copy.start()
         kz_sends.append(copy)
@@ -512,17 +527,15 @@
     def _():
         for i in range(2):
             slot = xt.at[i, core]
-            copy_to(slot, slot, s_z, r_z.at[i], s, near).wait_recv()
+            copy_to(slot, slot, sent, r_z.at[i], s, near).wait_recv()
             x_sends[i].start()
-        for copy in x_sends:
-            copy.wait_recv()
+        arrived(xt.at[:, core], r_xf)
 
     conv_block(0)
     for k in range(7, 10):
         relay(k)
 
-    for i, p in enumerate(tp_peers):
-        copy_to(qp.at[p], qp.at[p], s_q.at[i], r_q.at[i], s, p).wait_recv()
+    arrived(qp.at[pl.ds(0, n - 1)], r_q)
     q_float = [qp[j].astype(f32) for j in range(n)]
     qw = q_float[0].shape[1]
     q_square = sum(jnp.sum(q * q, axis=1, keepdims=True) for q in q_float)
@@ -541,21 +554,21 @@
     for k in (2, 1, 3):
         z = lax.rem(s + n - k, n)
         copy_to(
-            kvr.at[z, mine], kvr.at[z, mine], s_kz.at[k - 1], r_kz.at[k - 1], z, t
+            kvr.at[z, mine], kvr.at[z, mine], sent, r_kz.at[k - 1], z, t
         ).wait_recv()
         for i, p in enumerate(tp_peers):
             copy = copy_to(
-                kvr.at[z, mine], kvr.at[z, mine], s_kf.at[k - 1, i], r_kf.at[k - 1, i], s, p
+                kvr.at[z, mine], kvr.at[z, mine], sent, r_kf, s, p
             )
             copy.start()
             kf_sends.append(copy)
     conv_block(1)
     conv_block(2)
-    for k in (2, 1, 3):
-        z = lax.rem(s + n - k, n)
-        for i, p in enumerate(tp_peers):
-            rest = kvr.at[z, quarter(p)]
-            copy_to(rest, rest, s_kf.at[k - 1, i], r_kf.at[k - 1, i], s, p).wait_recv()
+    arrived(kvr.at[pl.ds(0, n - 1), pl.ds(0, (n - 1) * (rows // n))], r_kf)
+
+    @pl.when(is_hub)
+    def _():
+        gate_part()
 
     latent = jnp.concatenate([kvr[j, :, :lat] for j in range(n)], axis=0)
     ropes = jnp.concatenate([kvr[j, :, lat:] for j in range(n)], axis=0)
@@ -593,33 +606,13 @@
     for j in range(n):
         acc[j] = dot(y_attn, woa[j])
 
-    def take(m):
-        copy_to(part.at[0, m], got.at[m], s_p.at[0, m], r_p.at[m], s, near).wait_recv()
-        own[m] = own[m] + got[m].astype(f32)
-
-    take(2)
-    take(0)
-
-    def summed(i):
-        return (row_scale * own[i]).astype(bf16).astype(f32)
-
-    gated = (summed(2) * summed(0)).astype(bf16)
-    gate[...] = gated
-    edge = before.shape[0]
-    up = copy_to(gate.at[pl.ds(rows - edge, edge)], before, s_h.at[0], r_h.at[0], s + 1, t)
-    down = copy_to(gate.at[pl.ds(0, edge)], after, s_h.at[1], r_h.at[1], s - 1, t)
-
-    @pl.when(s < n - 1)
-    def _():
-        up.start()
-
-    @pl.when(s > 0)
-    def _():
-        down.start()
+    @pl.when(jnp.logical_not(is_hub))
+    def _():
+        gate_part()
 
     take(1)
     conv_outer = summed(1)
-    middle = gated.astype(f32)
+    middle = gate[...].astype(f32)
     kernel = [taps[i : i + 1, :].astype(f32) for i in range(3)]
     row = lax.broadcasted_iota(jnp.int32, middle.shape, 0)
     previous = pltpu.roll(middle, 1, 0)
@@ -652,15 +645,15 @@
         return acc[j] + dot(y_conv, woc[j])
 
     put_near[0] = share(diag).astype(bf16)
-    o_diag = copy_to(put_near.at[0], got_near.at[0], s_o.at[0], r_o.at[0], s, near)
+    o_diag = copy_to(put_near.at[0], got_near.at[0], sent, r_o.at[0], s, near)
     o_diag.start()
     far_share = share(far).astype(bf16).astype(f32)
     o_diag.wait_recv()
     put_far[...] = (far_share + got_near[0].astype(f32)).astype(bf16)
-    o_far = copy_to(put_far, got_far, s_o.at[1], r_o.at[1], s, far)
+    o_far = copy_to(put_far, got_far, sent, r_o.at[1], s, far)
     o_far.start()
     put_near[1] = share(near).astype(bf16)
-    o_near = copy_to(put_near.at[1], got_near.at[1], s_o.at[2], r_o.at[2], s, near)
+    o_near = copy_to(put_near.at[1], got_near.at[1], sent, r_o.at[2], s, near)
     o_near.start()
     my_share = share(t).astype(bf16).astype(f32)
     o_near.wait_recv()
@@ -777,13 +770,8 @@
         vm((rows, width), bf16),
     ]
     dma = pltpu.SemaphoreType.DMA
-    scratch += [dma((17 + 2 * n,)), dma((3,)), dma((3,)), dma, dma((2,))]
-    scratch += [dma((2,))] * 2
-    scratch += [dma((12,))] * 4
-    scratch += [dma((n - 1,))] * 6
-    scratch += [dma((n - 1, n - 1))] * 2
-    scratch += [dma((2, 3)), dma((3,))]
-    scratch += [dma((2,)), dma((2,)), dma((3,)), dma((3,))]
+    scratch += [dma((4,)), dma, dma((3,)), dma((2,)), dma, dma((12,)), dma((3,)), dma, dma]
+    scratch += [dma((n - 1,)), dma, dma((3,)), dma((2,)), dma((3,))]
     return pl.pallas_call(
         functools.partial(mixer_kernel, n),
         out_shape=pltpu.VMEM((rows, width), bf16),

time: 35.9 us -> 35 us (0.975)
  Pallas kernels: 35.1 us -> 34.2 us
    pallas_call x1, Pallas kernels: 35.1 us -> 34.2 us  [fused(): pl.pallas_call(functools.partial(mixer_kernel, n), out_shape=pltpu.VMEM((...]
where the time goes in v4:
time: 35 us; the launch traced here: 34.9 us
  Pallas kernels  34.2 us (98%)
  local copies, waits for them, and re-layouts  0.66 us (2%)
    pallas_call x1, Pallas kernels, fused(): pl.pallas_call(functools.partial(mixer_kernel, n), out_shape=pltpu.VMEM((...  34.2 us

profile of v4, /device:TPU:0, one launch (start us, length us, event | category | flops | bytes accessed | tf_op | source)
XLA Modules:
  0.0 34.9 jit_solution(17285527065271185487)
XLA Ops:
  0.0 34.2 %shard_map.181 = bf16[128,512]{1,0:T(8,128)(2,1)S(1)} custom-call(bf16[128,512]{1,0:T(8,128)(2,1)} %tokens_h.1, bf16[2048]{0:T(1024)(128)(2,1)} %gain_h.1, bf16[512,256]{1,0:T(8,128)(2,1)} %wcv_h.1, bf16[512,256]{1,0:T(8,128)(2,1)} %wco_h.1, bf16[512,256]{1,0:T(8,128)(2,1)} %wci_h.1, bf16[3,256]{1,0:T(4,128)(2,1)} %taps_h.1, bf16[4,512,128]{2,1,0:T(8,128)(2,1)} %bitcast.3, ...), custom_call_target="tpu_custom_call" | custom-call | tf_op jit(solution)/shard_map/pallas_call | solution.py:775
  34.2 0.7 %copy.21 = bf16[128,512]{1,0:T(8,128)(2,1)} copy(bf16[128,512]{1,0:T(8,128)(2,1)S(1)} %shard_map.181) | data formatting | bytes 262144

commit v5 on v4

--- a/solution.py
+++ b/solution.py
@@ -245,6 +245,7 @@
     qp,
     kvp,
     kvr,
+    rk,
     gate,
     before,
     after,
@@ -264,6 +265,7 @@
     r_kv,
     r_kz,
     r_kf,
+    r_rk,
     r_p,
     r_h,
     r_o,
@@ -379,6 +381,33 @@
         copy.start()
     for load in loads[1:5] + loads[8:]:
         load.wait()
+    def scaled_slice(block, f):
+        gain_f = gain[pl.ds(pl.multiple_of(f * width, width), width)][None, :].astype(f32)
+        return (block.astype(f32) * gain_f).astype(bf16)
+
+    def features(f):
+        return pl.ds(pl.multiple_of(f * width, width), width)
+
+    def square_sum(f):
+        piece = tok[f].astype(f32)
+        return jnp.sum(piece * piece, axis=1, keepdims=True)
+
+    def kv_product(scaled, f):
+        return dot_t(scaled, wkv[:, features(f)])
+
+    def r_product(scaled, f):
+        return dot_t(scaled, wr[:, features(f)])
+
+    def project(f):
+        scaled = scaled_slice(tok[f], f)
+        sums = (kv_product(scaled, f), r_product(scaled, f), dot(scaled, wq[f]))
+        return (square_sum(f),) + sums
+
+    squares, kv_sum, r_sum, q_sum = project(t)
+    copy_to(tok.at[near], tok.at[near], sent, r_tok.at[1], s, near).wait_recv()
+    more = project(near)
+    squares, kv_sum = squares + more[0], kv_sum + more[1]
+    r_sum, q_sum = r_sum + more[2], q_sum + more[3]
     copy_to(tok.at[far], tok.at[far], sent, r_tok.at[0], s, far).wait_recv()
     tok_fwd.start()
 
@@ -386,22 +415,15 @@
     def _():
         z_far.start()
 
-    for copy in w_sends[6:]:
+    for copy in w_sends[6:9]:
         copy.start()
-    copy_to(tok.at[near], tok.at[near], sent, r_tok.at[1], s, near).wait_recv()
+    more = project(far)
+    squares, kv_sum = squares + more[0], kv_sum + more[1]
+    r_sum, q_sum = r_sum + more[2], q_sum + more[3]
     copy_to(tok.at[diag], tok.at[diag], sent, r_tok.at[2], s, near).wait_recv()
-
-    squares = jnp.zeros((rows, 1), f32)
-    q_sum = jnp.zeros((rows, wq.shape[2]), f32)
-    kv_sum = jnp.zeros((rows, wkv.shape[0]), f32)
-    r_sum = jnp.zeros((rows, wr.shape[0]), f32)
-    for j in range(n):
-        piece = tok[j].astype(f32)
-        squares = squares + jnp.sum(piece * piece, axis=1, keepdims=True)
-        scaled = (piece * gain[j * width : (j + 1) * width][None, :].astype(f32)).astype(bf16)
-        kv_sum = kv_sum + dot_t(scaled, wkv[:, j * width : (j + 1) * width])
-        r_sum = r_sum + dot_t(scaled, wr[:, j * width : (j + 1) * width])
-        q_sum = q_sum + dot(scaled, wq[j])
+    last = scaled_slice(tok[diag], diag)
+    squares = squares + square_sum(diag)
+    kv_sum = kv_sum + kv_product(last, diag)
     row_scale = lax.rsqrt(squares / (n * width) + EPS)
     kw = wkv.shape[0]
     place = (
@@ -415,75 +437,14 @@
     ]
     for copy in (kv_sends[1], kv_sends[2], kv_sends[0]):
         copy.start()
+    q_sum = q_sum + dot(last, wq[diag])
+    r_sum = r_sum + r_product(last, diag)
     qp[t] = (row_scale * q_sum).astype(bf16)
     q_sends = [
         copy_to(qp.at[t], qp.at[t], sent, r_q, s, p) for i, p in enumerate(tp_peers)
     ]
     for copy in (q_sends[1], q_sends[2], q_sends[0]):
         copy.start()
-
-    def scaled_slice(block, f):
-        gain_f = gain[pl.ds(pl.multiple_of(f * width, width), width)][None, :].astype(f32)
-        return (block.astype(f32) * gain_f).astype(bf16)
-
-    mine_scaled = scaled_slice(tok[s], s)
-    for m in order:
-        own[m] = dot(mine_scaled, weights[m][...])
-    for k in range(4):
-        relay(k)
-
-    edge = before.shape[0]
-    up = copy_to(gate.at[pl.ds(rows - edge, edge)], before, sent, r_h.at[0], s + 1, t)
-    down = copy_to(gate.at[pl.ds(0, edge)], after, sent, r_h.at[1], s - 1, t)
-
-    def take(m):
-        arrived(got.at[m], r_p.at[m])
-        own[m] = own[m] + got[m].astype(f32)
-
-    def summed(i):
-        return (row_scale * own[i]).astype(bf16).astype(f32)
-
-    def gate_part():
-        take(2)
-        take(0)
-        gate[...] = (summed(2) * summed(0)).astype(bf16)
-
-        @pl.when(s < n - 1)
-        def _():
-            up.start()
-
-        @pl.when(s > 0)
-        def _():
-            down.start()
-
-    p_sends = []
-    for i in range(2):
-        for m in range(3):
-            target = hub_over if i else end_over
-            p_sends.append(
-                copy_to(part.at[i, m], got.at[m], sent, r_p.at[m], target, t)
-            )
-    x_sends = []
-    for i in range(2):
-        slot = xt.at[i, core]
-        x_sends.append(copy_to(slot, slot, sent, r_xf, s, near))
-
-    def conv_block(j):
-        m = order[j]
-        arrived(wx.at[m, pl.ds(0, wx.shape[1] // 2)], r_y.at[m])
-
-        @pl.when(is_hub)
-        def _():
-            first = jnp.concatenate([xt[i, lax.rem(s, 2)] for i in range(2)], axis=0)
-            second = jnp.concatenate([xt[i, lax.rem(mate, 2)] for i in range(2)], axis=0)
-            total = dot(scaled_slice(first, s), weights[m][...]) + dot(
-                scaled_slice(second, mate), wx[m]
-            )
-            for i in range(2):
-                part[i, m] = total[i * rows : (i + 1) * rows].astype(bf16)
-                p_sends[3 * i + m].start()
-
-        own[m] = own[m] + dot(scaled_slice(tok[mate], mate), wx[m])
 
     cos_v, sin_v = cosine[...], sine[...]
     lanes = cos_v.shape[1]
@@ -499,14 +460,84 @@
     spread = jnp.where(lax.rem(spread_c, ROPE) == spread_r, 1.0, 0.0).astype(bf16)
     rope_raw = dot((row_scale * r_sum).astype(bf16), spread).astype(bf16)
     k_rope = (rope_raw.astype(f32) * cos_v + dot(rope_raw, turn) * sin_v).astype(bf16)
+    groups = lanes // ROPE
+    slab = rows // groups
+    slab_lane = lax.div(lax.broadcasted_iota(jnp.int32, (slab, lanes), 1), ROPE)
+    packed = jnp.zeros((slab, lanes), f32)
+    for i in range(groups):
+        packed = jnp.where(slab_lane == i, k_rope[i * slab : (i + 1) * slab].astype(f32), packed)
+    rk[s] = packed.astype(bf16)
+    rk_sends = [
+        copy_to(rk.at[s], rk.at[s], sent, r_rk, lax.rem(s + k, n), t) for k in range(1, n)
+    ]
+    for copy in (rk_sends[1], rk_sends[0], rk_sends[2]):
+        copy.start()
+
+    mine_scaled = scaled_slice(tok[s], s)
+    for m in order:
+        own[m] = dot(mine_scaled, weights[m][...])
+    for k in range(4):
+        relay(k)
+
+    edge = before.shape[0]
+    up = copy_to(gate.at[pl.ds(rows - edge, edge)], before, sent, r_h.at[0], s + 1, t)
+    down = copy_to(gate.at[pl.ds(0, edge)], after, sent, r_h.at[1], s - 1, t)
+
+    def take(m):
+        arrived(got.at[m], r_p.at[m])
+        own[m] = own[m] + got[m].astype(f32)
+
+    def summed(i):
+        return (row_scale * own[i]).astype(bf16).astype(f32)
+
+    def gate_part():
+        take(2)
+        take(0)
+        gate[...] = (summed(2) * summed(0)).astype(bf16)
+
+        @pl.when(s < n - 1)
+        def _():
+            up.start()
+
+        @pl.when(s > 0)
+        def _():
+            down.start()
+
+    p_sends = []
+    for i in range(2):
+        for m in range(3):
+            target = hub_over if i else end_over
+            p_sends.append(
+                copy_to(part.at[i, m], got.at[m], sent, r_p.at[m], target, t)
+            )
+    x_sends = []
+    for i in range(2):
+        slot = xt.at[i, core]
+        x_sends.append(copy_to(slot, slot, sent, r_xf, s, near))
+
+    def conv_block(j):
+        m = order[j]
+        arrived(wx.at[m, pl.ds(0, wx.shape[1] // 2)], r_y.at[m])
+
+        @pl.when(is_hub)
+        def _():
+            first = jnp.concatenate([xt[i, lax.rem(s, 2)] for i in range(2)], axis=0)
+            second = jnp.concatenate([xt[i, lax.rem(mate, 2)] for i in range(2)], axis=0)
+            total = dot(scaled_slice(first, s), weights[m][...]) + dot(
+                scaled_slice(second, mate), wx[m]
+            )
+            for i in range(2):
+                part[i, m] = total[i * rows : (i + 1) * rows].astype(bf16)
+                p_sends[3 * i + m].start()
+
+        own[m] = own[m] + dot(scaled_slice(tok[mate], mate), wx[m])
+
     arrived(kvp.at[pl.ds(0, n - 1)], r_kv)
     kv_float = jnp.concatenate(
         [kvp[j].astype(f32) + kvp[j + 1].astype(f32) for j in range(0, n, 2)], axis=1
     )
     kv_scale = lax.rsqrt(jnp.mean(kv_float * kv_float, axis=1, keepdims=True) + EPS)
-    lat = kv_float.shape[1]
-    kvr[s, :, :lat] = (kv_float * kv_scale * kvg[...][None, :].astype(f32)).astype(bf16)
-    kvr[s, :, lat:] = k_rope
+    kvr[s] = (kv_float * kv_scale * kvg[...][None, :].astype(f32)).astype(bf16)
     def quarter(index):
         return pl.ds(pl.multiple_of(index * (rows // n), rows // n), rows // n)
 
@@ -519,8 +550,10 @@
         )
         copy.start()
         kz_sends.append(copy)
-
-    for k in range(4, 7):
+    for copy in w_sends[9:]:
+        copy.start()
+
+    for k in range(4, 8):
         relay(k)
 
     @pl.when(is_hub)
@@ -532,7 +565,7 @@
         arrived(xt.at[:, core], r_xf)
 
     conv_block(0)
-    for k in range(7, 10):
+    for k in range(8, 10):
         relay(k)
 
     arrived(qp.at[pl.ds(0, n - 1)], r_q)
@@ -570,8 +603,19 @@
     def _():
         gate_part()
 
-    latent = jnp.concatenate([kvr[j, :, :lat] for j in range(n)], axis=0)
-    ropes = jnp.concatenate([kvr[j, :, lat:] for j in range(n)], axis=0)
+    latent = jnp.concatenate(
+        [kvr[j, i * slab : (i + 1) * slab] for i in range(groups) for j in range(n)], axis=0
+    )
+    arrived(rk.at[pl.ds(0, n - 1)], r_rk)
+    packs = jnp.concatenate([rk[j] for j in range(n)], axis=0)
+    same = lax.rem(turn_r, ROPE) == lax.rem(turn_c, ROPE)
+    ropes = jnp.concatenate(
+        [
+            dot(packs, jnp.where(same & (lax.div(turn_r, ROPE) == i), 1.0, 0.0).astype(bf16))
+            for i in range(groups)
+        ],
+        axis=0,
+    ).astype(bf16)
     keys = dot(latent, wkn[...]).astype(bf16)
     values = dot(latent, wva[...]).astype(bf16)
     heads = wqn.shape[1] // NOPE
@@ -664,7 +708,7 @@
     tok_fwd.wait_send()
 
     z_own.wait_send()
-    for copy in kv_sends + q_sends + kz_sends + kf_sends + w_sends + y_sends:
+    for copy in kv_sends + q_sends + rk_sends + kz_sends + kf_sends + w_sends + y_sends:
         copy.wait_send()
 
     @pl.when(is_hub)
@@ -759,7 +803,8 @@
         vm((3, rows, cw), f32),
         vm((n, rows, w_q_down.shape[1]), bf16),
         vm((n, rows, 2 * w_kv_down.shape[1]), bf16),
-        vm((n, rows, lat + lanes), bf16),
+        vm((n, rows, lat), bf16),
+        vm((n, rows // heads, lanes), bf16),
         vm((rows, cw), bf16),
         vm((16, cw), bf16),
         vm((16, cw), bf16),
@@ -771,7 +816,7 @@
     ]
     dma = pltpu.SemaphoreType.DMA
     scratch += [dma((4,)), dma, dma((3,)), dma((2,)), dma, dma((12,)), dma((3,)), dma, dma]
-    scratch += [dma((n - 1,)), dma, dma((3,)), dma((2,)), dma((3,))]
+    scratch += [dma((n - 1,)), dma, dma, dma((3,)), dma((2,)), dma((3,))]
     return pl.pallas_call(
         functools.partial(mixer_kernel, n),
         out_shape=pltpu.VMEM((rows, width), bf16),

time: 35 us -> 33.8 us (0.966)
  Pallas kernels: 34.2 us -> 33 us
    pallas_call x1, Pallas kernels: 34.2 us -> 33 us  [fused(): pl.pallas_call(functools.partial(mixer_kernel, n), out_shape=pltpu.VMEM((...]
where the time goes in v5:
time: 33.8 us; the launch traced here: 33.7 us
  Pallas kernels  33 us (98%)
  local copies, waits for them, and re-layouts  0.66 us (2%)
    pallas_call x1, Pallas kernels, fused(): pl.pallas_call(functools.partial(mixer_kernel, n), out_shape=pltpu.VMEM((...  33 us

profile of v5, /device:TPU:0, one launch (start us, length us, event | category | flops | bytes accessed | tf_op | source)
XLA Modules:
  0.0 33.7 jit_solution(17847964643162120355)
XLA Ops:
  0.0 33.0 %shard_map.181 = bf16[128,512]{1,0:T(8,128)(2,1)S(1)} custom-call(bf16[128,512]{1,0:T(8,128)(2,1)} %tokens_h.1, bf16[2048]{0:T(1024)(128)(2,1)} %gain_h.1, bf16[512,256]{1,0:T(8,128)(2,1)} %wcv_h.1, bf16[512,256]{1,0:T(8,128)(2,1)} %wco_h.1, bf16[512,256]{1,0:T(8,128)(2,1)} %wci_h.1, bf16[3,256]{1,0:T(4,128)(2,1)} %taps_h.1, bf16[4,512,128]{2,1,0:T(8,128)(2,1)} %bitcast.3, ...), custom_call_target="tpu_custom_call" | custom-call | tf_op jit(solution)/shard_map/pallas_call | solution.py:820
  33.0 0.7 %copy.21 = bf16[128,512]{1,0:T(8,128)(2,1)} copy(bf16[128,512]{1,0:T(8,128)(2,1)S(1)} %shard_map.181) | data formatting | bytes 262144

commit v6 on v5

--- a/solution.py
+++ b/solution.py
@@ -239,6 +239,9 @@
     sine,
     wx,
     xt,
+    xs,
+    base,
+    mine_other,
     part,
     got,
     own,
@@ -254,6 +257,7 @@
     got_near,
     put_far,
     got_far,
+    got_early,
     load_sem,
     sent,
     r_tok,
@@ -415,7 +419,7 @@
     def _():
         z_far.start()
 
-    for copy in w_sends[6:9]:
+    for copy in w_sends[6:10]:
         copy.start()
     more = project(far)
     squares, kv_sum = squares + more[0], kv_sum + more[1]
@@ -515,22 +519,35 @@
         slot = xt.at[i, core]
         x_sends.append(copy_to(slot, slot, sent, r_xf, s, near))
 
+    def conv_start():
+        @pl.when(is_hub)
+        def _():
+            for i in range(2):
+                piece_rows = pl.ds(i * rows, rows)
+                xs[0, piece_rows] = scaled_slice(xt[i, lax.rem(s, 2)], s)
+                xs[1, piece_rows] = scaled_slice(xt[i, lax.rem(mate, 2)], mate)
+            base[order[0]] = dot(xs[0], weights[order[0]][...])
+
+    def conv_ahead():
+        @pl.when(is_hub)
+        def _():
+            for m in order[1:]:
+                base[m] = dot(xs[0], weights[m][...])
+
+        mine_other[...] = scaled_slice(tok[mate], mate)
+
     def conv_block(j):
         m = order[j]
         arrived(wx.at[m, pl.ds(0, wx.shape[1] // 2)], r_y.at[m])
 
         @pl.when(is_hub)
         def _():
-            first = jnp.concatenate([xt[i, lax.rem(s, 2)] for i in range(2)], axis=0)
-            second = jnp.concatenate([xt[i, lax.rem(mate, 2)] for i in range(2)], axis=0)
-            total = dot(scaled_slice(first, s), weights[m][...]) + dot(
-                scaled_slice(second, mate), wx[m]
-            )
-            for i in range(2):
+            total = base[m] + dot(xs[1], wx[m])
+            for i in (0, 1) if j == 2 else (1, 0):
                 part[i, m] = total[i * rows : (i + 1) * rows].astype(bf16)
                 p_sends[3 * i + m].start()
 
-        own[m] = own[m] + dot(scaled_slice(tok[mate], mate), wx[m])
+        own[m] = own[m] + dot(mine_other[...], wx[m])
 
     arrived(kvp.at[pl.ds(0, n - 1)], r_kv)
     kv_float = jnp.concatenate(
@@ -550,20 +567,29 @@
         )
         copy.start()
         kz_sends.append(copy)
-    for copy in w_sends[9:]:
+    for copy in w_sends[10:]:
         copy.start()
 
-    for k in range(4, 8):
-        relay(k)
-
-    @pl.when(is_hub)
-    def _():
-        for i in range(2):
+    def pass_on(i):
+        @pl.when(is_hub)
+        def _():
             slot = xt.at[i, core]
             copy_to(slot, slot, sent, r_z.at[i], s, near).wait_recv()
             x_sends[i].start()
+
+    relay(4)
+    relay(5)
+    pass_on(0)
+    pass_on(1)
+    relay(6)
+    relay(7)
+
+    @pl.when(is_hub)
+    def _():
         arrived(xt.at[:, core], r_xf)
 
+    conv_start()
+    conv_ahead()
     conv_block(0)
     for k in range(8, 10):
         relay(k)
@@ -688,13 +714,20 @@
     def share(j):
         return acc[j] + dot(y_conv, woc[j])
 
+    early = got_early.shape[0]
+    lead, rest = pl.ds(0, early), pl.ds(early, rows - early)
     put_near[0] = share(diag).astype(bf16)
-    o_diag = copy_to(put_near.at[0], got_near.at[0], sent, r_o.at[0], s, near)
+    o_diag = copy_to(put_near.at[0, rest], got_near.at[0, rest], sent, r_o.at[0], s, near)
     o_diag.start()
+    o_cross = copy_to(put_near.at[0, lead], got_early, sent, r_o.at[3], s, diag)
+    o_cross.start()
     far_share = share(far).astype(bf16).astype(f32)
+    put_far[lead] = far_share[:early].astype(bf16)
+    o_lead = copy_to(put_far.at[lead], got_far.at[lead], sent, r_o.at[1], s, far)
+    o_lead.start()
     o_diag.wait_recv()
-    put_far[...] = (far_share + got_near[0].astype(f32)).astype(bf16)
-    o_far = copy_to(put_far, got_far, sent, r_o.at[1], s, far)
+    put_far[rest] = (far_share[early:] + got_near[0, rest].astype(f32)).astype(bf16)
+    o_far = copy_to(put_far.at[rest], got_far.at[rest], sent, r_o.at[1], s, far)
     o_far.start()
     put_near[1] = share(near).astype(bf16)
     o_near = copy_to(put_near.at[1], got_near.at[1], sent, r_o.at[2], s, near)
@@ -724,10 +757,13 @@
     def _():
         down.wait_send()
 
-    o_diag.wait_send()
-    o_near.wait_send()
-    o_far.wait()
-    out_ref[...] = (my_share + got_far[...].astype(f32)).astype(bf16)
+    for copy in (o_diag, o_cross, o_lead, o_near, o_far):
+        copy.wait_send()
+    arrived(got_early, r_o.at[3])
+    arrived(got_far, r_o.at[1])
+    my_share = my_share + got_far[...].astype(f32)
+    out_ref[rest] = my_share[early:].astype(bf16)
+    out_ref[lead] = (my_share[:early] + got_early[...].astype(f32)).astype(bf16)
 
 
 def fits(grp, sp, tp, tokens, mix_gain, w_conv_value, *others):
@@ -798,6 +834,9 @@
     scratch += [
         vm((3,) + w_conv_value.shape, bf16),
         vm((2, 2, rows, width), bf16),
+        vm((2, 2 * rows, width), bf16),
+        vm((3, 2 * rows, cw), f32),
+        vm((rows, width), bf16),
         vm((2, 3, rows, cw), bf16),
         vm((3, rows, cw), bf16),
         vm((3, rows, cw), f32),
@@ -813,10 +852,11 @@
         vm((2, rows, width), bf16),
         vm((rows, width), bf16),
         vm((rows, width), bf16),
+        vm((rows // 8, width), bf16),
     ]
     dma = pltpu.SemaphoreType.DMA
     scratch += [dma((4,)), dma, dma((3,)), dma((2,)), dma, dma((12,)), dma((3,)), dma, dma]
-    scratch += [dma((n - 1,)), dma, dma, dma((3,)), dma((2,)), dma((3,))]
+    scratch += [dma((n - 1,)), dma, dma, dma((3,)), dma((2,)), dma((4,))]
     return pl.pallas_call(
         functools.partial(mixer_kernel, n),
         out_shape=pltpu.VMEM((rows, width), bf16),

time: 33.8 us -> 33.6 us (level)
  no operation moved by 1% of the time
where the time goes in v6:
time: 33.6 us; the launch traced here: 33.5 us
  Pallas kernels  32.8 us (98%)
  local copies, waits for them, and re-layouts  0.66 us (2%)
    pallas_call x1, Pallas kernels, fused(): pl.pallas_call(functools.partial(mixer_kernel, n), out_shape=pltpu.VMEM((...  32.8 us

profile of v6, /device:TPU:0, one launch (start us, length us, event | category | flops | bytes accessed | tf_op | source)
XLA Modules:
  0.0 33.5 jit_solution(3736766767718775206)
XLA Ops:
  0.0 32.8 %shard_map.181 = bf16[128,512]{1,0:T(8,128)(2,1)S(1)} custom-call(bf16[128,512]{1,0:T(8,128)(2,1)} %tokens_h.1, bf16[2048]{0:T(1024)(128)(2,1)} %gain_h.1, bf16[512,256]{1,0:T(8,128)(2,1)} %wcv_h.1, bf16[512,256]{1,0:T(8,128)(2,1)} %wco_h.1, bf16[512,256]{1,0:T(8,128)(2,1)} %wci_h.1, bf16[3,256]{1,0:T(4,128)(2,1)} %taps_h.1, bf16[4,512,128]{2,1,0:T(8,128)(2,1)} %bitcast.3, ...), custom_call_target="tpu_custom_call" | custom-call | tf_op jit(solution)/shard_map/pallas_call | solution.py:860
  32.8 0.7 %copy.21 = bf16[128,512]{1,0:T(8,128)(2,1)} copy(bf16[128,512]{1,0:T(8,128)(2,1)S(1)} %shard_map.181) | data formatting | bytes 262144

commit v7 on v6

--- a/solution.py
+++ b/solution.py
@@ -381,7 +381,7 @@
     def _():
         z_own.start()
 
-    for copy in w_sends[4:6]:
+    for copy in w_sends[4:7]:
         copy.start()
     for load in loads[1:5] + loads[8:]:
         load.wait()
@@ -419,7 +419,7 @@
     def _():
         z_far.start()
 
-    for copy in w_sends[6:10]:
+    for copy in w_sends[7:10]:
         copy.start()
     more = project(far)
     squares, kv_sum = squares + more[0], kv_sum + more[1]
@@ -542,10 +542,17 @@
 
         @pl.when(is_hub)
         def _():
-            total = base[m] + dot(xs[1], wx[m])
-            for i in (0, 1) if j == 2 else (1, 0):
-                part[i, m] = total[i * rows : (i + 1) * rows].astype(bf16)
-                p_sends[3 * i + m].start()
+            if j == 2:
+                for i in range(2):
+                    block = pl.ds(i * rows, rows)
+                    total = base[m, block] + dot(xs[1, block], wx[m])
+                    part[i, m] = total.astype(bf16)
+                    p_sends[3 * i + m].start()
+            else:
+                total = base[m] + dot(xs[1], wx[m])
+                for i in (1, 0):
+                    part[i, m] = total[i * rows : (i + 1) * rows].astype(bf16)
+                    p_sends[3 * i + m].start()
 
         own[m] = own[m] + dot(mine_other[...], wx[m])
 

time: 33.6 us -> 33.6 us (level)
  no operation moved by 1% of the time
where the time goes in v7:
time: 33.6 us; the launch traced here: 33.4 us
  Pallas kernels  32.8 us (98%)
  local copies, waits for them, and re-layouts  0.66 us (2%)
    pallas_call x1, Pallas kernels, fused(): pl.pallas_call(functools.partial(mixer_kernel, n), out_shape=pltpu.VMEM((...  32.8 us

profile of v7, /device:TPU:0, one launch (start us, length us, event | category | flops | bytes accessed | tf_op | source)
XLA Modules:
  0.0 33.4 jit_solution(27741059532808113)
XLA Ops:
  0.0 32.8 %shard_map.181 = bf16[128,512]{1,0:T(8,128)(2,1)S(1)} custom-call(bf16[128,512]{1,0:T(8,128)(2,1)} %tokens_h.1, bf16[2048]{0:T(1024)(128)(2,1)} %gain_h.1, bf16[512,256]{1,0:T(8,128)(2,1)} %wcv_h.1, bf16[512,256]{1,0:T(8,128)(2,1)} %wco_h.1, bf16[512,256]{1,0:T(8,128)(2,1)} %wci_h.1, bf16[3,256]{1,0:T(4,128)(2,1)} %taps_h.1, bf16[4,512,128]{2,1,0:T(8,128)(2,1)} %bitcast.3, ...), custom_call_target="tpu_custom_call" | custom-call | tf_op jit(solution)/shard_map/pallas_call | solution.py:867
  32.8 0.7 %copy.21 = bf16[128,512]{1,0:T(8,128)(2,1)} copy(bf16[128,512]{1,0:T(8,128)(2,1)S(1)} %shard_map.181) | data formatting | bytes 262144

commit v8 on v7

--- a/solution.py
+++ b/solution.py
@@ -381,7 +381,7 @@
     def _():
         z_own.start()
 
-    for copy in w_sends[4:7]:
+    for copy in w_sends[4:6]:
         copy.start()
     for load in loads[1:5] + loads[8:]:
         load.wait()
@@ -419,8 +419,16 @@
     def _():
         z_far.start()
 
-    for copy in w_sends[7:10]:
+    first_part = (12, 10)
+    for copy in w_sends[6 : min(first_part)]:
         copy.start()
+    for c in range(2):
+
+        @pl.when(core == c)
+        def _():
+            for copy in w_sends[min(first_part) : first_part[c]]:
+                copy.start()
+
     more = project(far)
     squares, kv_sum = squares + more[0], kv_sum + more[1]
     r_sum, q_sum = r_sum + more[2], q_sum + more[3]
@@ -574,8 +582,13 @@
         )
         copy.start()
         kz_sends.append(copy)
-    for copy in w_sends[10:]:
-        copy.start()
+    for c in range(2):
+
+        @pl.when(core == c)
+        def _():
+            for copy in w_sends[first_part[c] :]:
+                copy.start()
+
 
     def pass_on(i):
         @pl.when(is_hub)

time: 33.6 us -> 33.5 us (level)
  no operation moved by 1% of the time
where the time goes in v8:
time: 33.5 us; the launch traced here: 33.4 us
  Pallas kernels  32.7 us (98%)
  local copies, waits for them, and re-layouts  0.66 us (2%)
    pallas_call x1, Pallas kernels, fused(): pl.pallas_call(functools.partial(mixer_kernel, n), out_shape=pltpu.VMEM((...  32.7 us

profile of v8, /device:TPU:0, one launch (start us, length us, event | category | flops | bytes accessed | tf_op | source)
XLA Modules:
  0.0 33.4 jit_solution(14261921620168809567)
XLA Ops:
  0.0 32.7 %shard_map.181 = bf16[128,512]{1,0:T(8,128)(2,1)S(1)} custom-call(bf16[128,512]{1,0:T(8,128)(2,1)} %tokens_h.1, bf16[2048]{0:T(1024)(128)(2,1)} %gain_h.1, bf16[512,256]{1,0:T(8,128)(2,1)} %wcv_h.1, bf16[512,256]{1,0:T(8,128)(2,1)} %wco_h.1, bf16[512,256]{1,0:T(8,128)(2,1)} %wci_h.1, bf16[3,256]{1,0:T(4,128)(2,1)} %taps_h.1, bf16[4,512,128]{2,1,0:T(8,128)(2,1)} %bitcast.3, ...), custom_call_target="tpu_custom_call" | custom-call | tf_op jit(solution)/shard_map/pallas_call | solution.py:880
  32.7 0.7 %copy.21 = bf16[128,512]{1,0:T(8,128)(2,1)} copy(bf16[128,512]{1,0:T(8,128)(2,1)S(1)} %shard_map.181) | data formatting | bytes 262144
